TPU v7x, 256 devices: a 4x2x16 block of a 4x16x16 slice. The times are simulated.
256 devices in a mesh: grp: 2 (over y), sp: 32 (over z, core), tp: 4 (over x).
Axes of the slice: x: 4, y: 2, z: 16, core: 2. Of those that a mesh axis runs over, the one named last changes fastest.
The devices are a block of a 4x16x16 slice.
Arguments:
- residual: bfloat16 [16384, 2048], P(('grp', 'sp')), parts along dimension 0, may hold values from -6 to 6
- queries: bfloat16 [16384, 1024], P(('grp', 'sp'), 'tp'), parts along dimension 0, may hold values from -400 to 400
- keys: bfloat16 [16384, 1024], P(('grp', 'sp'), 'tp'), parts along dimension 0, may hold values from -8 to 8
- values: bfloat16 [16384, 1024], P(('grp', 'sp'), 'tp'), parts along dimension 0, may hold values from -6 to 6
- log_gates: float32 [16384, 16], P(('grp', 'sp'), 'tp'), parts along dimension 0, may hold values from -955 to 0, as said below
- w_out: bfloat16 [1024, 2048], P('tp'), may hold values from -0.75 to 0.75
- norm_gain: float32 [2048], replicated, may hold values from 0.1 to 1.9
- w_gate: bfloat16 [2048, 5632], P('sp', 'tp'), may hold values from -0.125 to 0.125
- w_up: bfloat16 [2048, 5632], P('sp', 'tp'), may hold values from -0.125 to 0.125
- w_down: bfloat16 [5632, 2048], P('tp', 'sp'), may hold values from -0.078125 to 0.078125
Outputs:
- output: bfloat16 [16384, 2048], P(('grp', 'sp', 'tp')), parts along dimension 0
There are 2 independent parts, one for each index of `grp`. A program takes and returns all parts, laid end to end along the dimension named above; an argument that names none is the same for every part. Nothing has to cross between parts.
Inputs may be any that keep to these rules, and one draw needn't show every extreme that they name: `log_gates`: never rises along positions.
All inputs are finite; a program needn't handle non-finite values.
Results may differ from a plain program's by a relative error of at most 0.014.
Values may be sent and summed in bfloat16 or wider, within the bound.
A program may use at most 128 MiB of HBM per device.

v0:
```python
import math

import jax
import jax.numpy as jnp
from jax import lax
from jax.sharding import PartitionSpec as P


def turned_gather(arrays, axis, dims):
    turned = [jnp.moveaxis(a, dim, 0) for a, dim in zip(arrays, dims)]
    widths = [t[0].size for t in turned]
    both = jnp.concatenate([t.reshape(-1, w) for t, w in zip(turned, widths)], axis=1)
    result = lax.all_gather(both, axis, axis=0, tiled=True)
    parts = jnp.split(result, [sum(widths[:k]) for k in range(1, len(widths))], axis=1)
    return tuple(
        (
            jnp.moveaxis(b.reshape(-1, *t.shape[1:]), 0, dim)
            for b, t, dim in zip(parts, turned, dims)
        )
    )


def cut_along(value, dim, peers):
    before, after = (value.shape[:dim], value.shape[dim + 1 :])
    return jnp.moveaxis(value.reshape(*before, peers, -1, *after), dim, 0)


def sent_and_summed(value, axis, dim):
    parts = cut_along(value, dim, lax.axis_size(axis))
    arrived = lax.all_to_all(parts, axis, split_axis=0, concat_axis=0, tiled=True)
    return arrived.astype(jnp.float32).sum(axis=0)


def sent_to_all(value, axis):
    copies = jnp.broadcast_to(value, (lax.axis_size(axis), *value.shape))
    return lax.all_to_all(copies, axis, split_axis=0, concat_axis=0, tiled=True)


def laid_out(parts, dim):
    parts = jnp.moveaxis(parts, 0, dim)
    dims = parts.shape
    return parts.reshape(*dims[:dim], dims[dim] * dims[dim + 1], *dims[dim + 2 :])


def gather_directly(value, axis, dim):
    parts = sent_to_all(value, axis)
    return laid_out(parts, dim)


def normalize(rows_in, gain):
    floats = rows_in.astype(jnp.float32)
    scaled = floats * lax.rsqrt(jnp.mean(floats * floats, axis=-1, keepdims=True) + 1e-06)
    return (scaled * gain).astype(jnp.bfloat16)


def attend(queries, keys, values, log_gates):
    row_count = queries.shape[0]
    head_count = log_gates.shape[1]
    head_width = queries.shape[1] // head_count
    score_scale = head_width ** (-0.5)
    first_row = lax.axis_index("sp") * row_count
    query_heads = queries.reshape(row_count, head_count, head_width)
    query_gates = log_gates.T
    query_positions = first_row + jnp.arange(row_count, dtype=jnp.int32)
    initial = (
        jnp.full((head_count, row_count), -1e30, jnp.float32),
        jnp.zeros((head_count, row_count), jnp.float32),
        jnp.zeros((head_count, row_count, head_width), jnp.float32),
    )
    carried = initial
    key_piece = lax.all_gather(keys.astype(jnp.float32), "sp", axis=0, tiled=True).astype(
        jnp.bfloat16
    )
    value_piece = lax.all_gather(values.astype(jnp.float32), "sp", axis=0, tiled=True).astype(
        jnp.bfloat16
    )
    gate_piece = lax.all_gather(log_gates, "sp", axis=0, tiled=True)
    length = key_piece.shape[0]
    block_rows = math.gcd(length, 2048)
    block_count = length // block_rows
    key_blocks = key_piece.reshape(block_count, block_rows, head_count, head_width)
    value_blocks = value_piece.reshape(block_count, block_rows, head_count, head_width)
    gate_blocks = gate_piece.reshape(block_count, block_rows, head_count)
    offsets = jnp.arange(block_count, dtype=jnp.int32) * block_rows

    def one_block(state, inputs):
        current_key_block, value_block, gate_block, offset = inputs

        def work(current):
            running_max, running_sum, accumulated = current
            scores = (
                jnp.einsum(
                    "qhd,khd->hqk",
                    query_heads,
                    current_key_block,
                    preferred_element_type=jnp.float32,
                )
                * score_scale
            )
            scores = scores + query_gates[:, :, None] - gate_block.T[:, None, :]
            key_positions = offset + jnp.arange(block_rows, dtype=jnp.int32)
            causal = (query_positions[:, None] >= key_positions[None, :])[None]
            scores = jnp.where(causal, scores, -1e30)
            new_max = jnp.maximum(running_max, jnp.max(scores, axis=-1))
            weights = jnp.where(causal, jnp.exp(scores - new_max[:, :, None]), 0.0)
            rescale = jnp.exp(running_max - new_max)
            running_sum = running_sum * rescale + jnp.sum(weights, axis=-1)
            product = jnp.einsum(
                "hqk,khd->hqd",
                weights.astype(jnp.bfloat16),
                value_block,
                preferred_element_type=jnp.float32,
            )
            accumulated = accumulated * rescale[:, :, None] + product
            return (new_max, running_sum, accumulated)

        state = lax.cond(offset <= first_row + row_count - 1, work, lambda current: current, state)
        return (state, None)

    carried, _ = lax.scan(one_block, carried, (key_blocks, value_blocks, gate_blocks, offsets))
    running_max, running_sum, accumulated = carried
    attended = accumulated / running_sum[:, :, None]
    return (
        attended.transpose(1, 0, 2).reshape(row_count, head_count * head_width).astype(jnp.bfloat16)
    )


def body(residual, queries, keys, values, log_gates, w_out, norm_gain, w_gate, w_up, w_down):
    gate_whole, up_whole, down_whole = turned_gather((w_gate, w_up, w_down), "sp", (0, 0, 1))
    attended = attend(queries, keys, values, log_gates)
    row_count = attended.shape[0]
    per_device = row_count // lax.axis_size("tp")
    my_first = lax.axis_index("tp") * per_device
    rows_part = attended
    projected = sent_and_summed(
        jnp.dot(rows_part, w_out, preferred_element_type=jnp.float32).astype(jnp.bfloat16), "tp", 0
    )
    own_rows = lax.dynamic_slice_in_dim(residual, my_first, per_device, 0)
    mixed = (own_rows.astype(jnp.float32) + projected).astype(jnp.bfloat16)
    normed_all = gather_directly(normalize(mixed, norm_gain), "tp", 0)
    gate_proj = jnp.dot(normed_all, gate_whole, preferred_element_type=jnp.float32)
    up_proj = jnp.dot(normed_all, up_whole, preferred_element_type=jnp.float32)
    hidden = (jax.nn.silu(gate_proj) * up_proj).astype(jnp.bfloat16)
    rows_part = hidden
    down_sum = sent_and_summed(
        jnp.dot(rows_part, down_whole, preferred_element_type=jnp.float32).astype(jnp.bfloat16),
        "tp",
        0,
    )
    summed = mixed.astype(jnp.float32) + 0.5 * down_sum
    scaled = summed * lax.rsqrt(jnp.mean(summed * summed, axis=-1, keepdims=True) + 1e-06)
    return scaled.astype(jnp.bfloat16)


def solution(mesh):
    in_specs = (
        P(("grp", "sp"), None),
        P(("grp", "sp"), "tp"),
        P(("grp", "sp"), "tp"),
        P(("grp", "sp"), "tp"),
        P(("grp", "sp"), "tp"),
        P("tp", None),
        P(),
        P("sp", "tp"),
        P("sp", "tp"),
        P("tp", "sp"),
    )
    out_specs = P(("grp", "sp", "tp"), None)
    return jax.shard_map(body, mesh=mesh, in_specs=in_specs, out_specs=out_specs, check_vma=False)
```

profile of v0, /device:TPU:33, one launch (start us, length us, event | category | flops | bytes accessed | tf_op | source)
XLA Modules:
  0.0 313.2 jit_solution(8759810375416187780)
XLA Ops:
  6.5 0.0 copy-start
  6.6 0.0 all-gather.4.cloned.1.call-start
  6.6 0.7 all-gather.4.cloned.1.call-update
  7.3 0.1 all-gather.6.cloned.1.call-start
  7.4 0.7 all-gather.6.cloned.1.call-update
  8.1 0.1 all-gather.8.cloned.1.call-start
  8.2 2.0 pad_maximum_fusion
  10.1 0.1 all-gather.8.cloned.1.call-update
  10.2 1.0 copy.15
  11.2 51.1 %all_gather.13 = f32[8192,4]{0,1:T(4,128)S(1)} all-gather(f32[256,4]{0,1:T(4,128)} %param.18), channel_id=1, replica_groups=mesh['grp'=2,'sp'=32,'tp'=4] {'sp'}, dimensions={0}, use_global_device_ids=true | all-gather | bytes 135168 | tf_op jit(solution)/shard_map/all_gather | solution.py:77
  62.3 33.5 %all-gather.4.cloned.1.call-done = bf16[8192,256]{1,0:T(8,128)(2,1)} async-done(((bf16[256,256]{1,0:T(8,128)(2,1)}), bf16[8192,256]{1,0:T(8,128)(2,1)}) %all-gather.4.cloned.1.call-update) | async-done | bytes 4194320 | tf_op jit(solution)/shard_map/all_gather | solution.py:71
  95.8 12.9 %reshape.83 = bf16[4,2048,4,64]{3,2,1,0:T(4,128)(2,1)} reshape(bf16[8192,256]{1,0:T(8,128)(2,1)} %all-gather.4.cloned.1.call-done) | data formatting | bytes 8388608 | tf_op jit(solution)/shard_map/reshape | solution.py:81
  108.7 12.9 %copy.17 = bf16[4,2048,4,64]{1,3,2,0:T(8,128)(2,1)} copy(bf16[4,2048,4,64]{3,2,1,0:T(4,128)(2,1)} %reshape.83) | data formatting | bytes 8388608
  121.6 45.0 %all-gather.6.cloned.1.call-done = bf16[8192,256]{1,0:T(8,128)(2,1)} async-done(((bf16[256,256]{1,0:T(8,128)(2,1)}), bf16[8192,256]{1,0:T(8,128)(2,1)}) %all-gather.6.cloned.1.call-update) | async-done | bytes 4194320 | tf_op jit(solution)/shard_map/all_gather | solution.py:74
  166.6 12.9 %reshape.84 = bf16[4,2048,4,64]{3,2,1,0:T(4,128)(2,1)} reshape(bf16[8192,256]{1,0:T(8,128)(2,1)} %all-gather.6.cloned.1.call-done) | data formatting | bytes 8388608 | tf_op jit(solution)/shard_map/reshape | solution.py:82
  179.5 0.0 copy-start.1
  179.5 13.0 %copy.18 = bf16[4,2048,4,64]{1,3,2,0:T(8,128)(2,1)} copy(bf16[4,2048,4,64]{3,2,1,0:T(4,128)(2,1)} %reshape.84) | data formatting | bytes 8388608
  192.5 0.0 copy-done.1
  192.5 0.0 copy-start.2
  192.5 18.0 %while.17 = (s32[]{:T(128)}, f32[4,256]{1,0:T(4,128)S(1)}, f32[4,256]{1,0:T(4,128)S(1)}, f32[4,256,64]{1,2,0:T(8,128)S(1)}, s32[4]{0:T(128)S(1)}, /*index=5*/s32...) while((s32[]{:T(128)}, f32[4,256]{1,0:T(4,128)S(1)}, ...), condition=%wide.region_5.6_spmd.clone, body=%wide.region_0.5_spmd.clone.sunk | while | flops 577376512 | bytes 30278972 | solution.py:120
  192.6 0.7 dynamic_slice.54
  193.9 12.6 %conditional.3 = ((f32[4,256]{1,0:T(4,128)S(1)}, f32[4,256]{1,0:T(4,128)S(1)}, f32[4,256,64]{1,2,0:T(8,128)S(1)})) conditional(s32[]{:T(128)} %convert_element_type.112, (f32[4,256]{1,0:T(4,128)S(1)}, f32[4,256]{1,0:T(4,128)S(1)}, f32[4,256,64]{1,2,0:T(8,128)S(1)}) %tuple.48, (s32[]{:T(128)}, s32[]{:T(128)}, bf16[4,2048,4,64]{1,3,2,0:T(8,128)(2,1)}, ...), branch_computations={%region_1.1_spmd, %region_2.4_spmd} | conditional | flops 577376512 | bytes 30277676 | solution.py:117
  193.9 0.7 iota_add_fusion
  194.6 0.5 broadcast_compare_fusion
  195.1 4.2 %fusion.4 = (f32[4,256]{1,0:T(4,128)S(1)}, f32[4,2048,256]{2,1,0:T(8,128)S(1)}) fusion(f32[4,2048]{1,0:T(4,128)S(1)} %dynamic-slice_bitcast_fusion, f32[4,256]{1,0:T(4,128)S(1)} %get-tuple-element.229, pred[256,2048]{0,1:T(8,128)(4,1)S(1)} %broadcast_compare_fusion, bf16[256,4,64]{0,2,1:T(8,128)(2,1)S(1)} %get-tuple-element.228, ...), kind=kOutput, calls=%fused_computation.5 | convolution fusion | flops 278920192 | bytes 10134016 | tf_op jit(solution)/shard_map/while/body/eval_jaxpr/cond/branch_1_fun/qhd,khd->hqk/dot_general | solution.py:92
  199.3 2.9 fusion.3
  202.3 4.2 %fusion.8 = f32[4,256,64]{1,2,0:T(8,128)S(1)} fusion(f32[4,2048,256]{2,1,0:T(8,128)S(1)} %get-tuple-element.328, f32[4,256]{1,0:T(4,128)S(1)} %max.4, f32[4,2048]{1,0:T(4,128)S(1)} %dynamic-slice_bitcast_fusion, f32[4,256]{1,0:T(4,128)S(1)} %get-tuple-element.229, pred[256,2048]{0,1:T(8,128)(4,1)S(1)} %broadcast_compare_fusion, ...), kind=kOutput, calls=%fused_computation.8 | convolution fusion | flops 283246592 | bytes 10531328 | tf_op jit(solution)/shard_map/while/body/eval_jaxpr/cond/branch_1_fun/hqk,khd->hqd/dot_general | solution.py:108
  206.5 0.7 dynamic_slice.54
  207.9 0.7 dynamic_slice.54
  209.2 0.7 dynamic_slice.54
  210.6 0.0 copy-done
  210.6 1.4 convolution_convert_fusion
  212.1 3.7 %all-to-all-start = ((bf16[4,64,2048]{2,1,0:T(8,128)(2,1)}), bf16[4,64,2048]{2,1,0:T(8,128)(2,1)S(1)}, u32[]{:S(2)}, u32[]{:S(2)}) async-start(bf16[4,64,2048]{2,1,0:T(8,128)(2,1)} %bitcast.10), calls=%async_computation | async-start | bytes 2097152 | tf_op jit(solution)/shard_map/all_to_all | solution.py:30
  215.8 14.6 %all-to-all-done = bf16[4,64,2048]{2,1,0:T(8,128)(2,1)S(1)} async-done(((bf16[4,64,2048]{2,1,0:T(8,128)(2,1)}), bf16[4,64,2048]{2,1,0:T(8,128)(2,1)S(1)}, u32[]{:S(2)}, u32[]{:S(2)}) %all-to-all-start) | async-done | bytes 1048608 | tf_op jit(solution)/shard_map/all_to_all | solution.py:30
  230.4 0.2 convert_reduce_fusion.1
  230.5 1.1 fusion.44
  231.7 0.0 copy-done.2
  231.7 0.1 fusion.46
  231.8 0.1 broadcast_in_dim.51
  232.0 15.9 %all_to_all.15 = bf16[4,64,2048]{2,1,0:T(8,128)(2,1)S(1)} all-to-all(bf16[4,64,2048]{2,1,0:T(8,128)(2,1)S(1)} %broadcast_in_dim.51), channel_id=1, replica_groups=mesh['grp'=2,'sp'=32,'tp'=4] {'tp'}, dimensions={0} | all-to-all | bytes 2097152 | tf_op jit(solution)/shard_map/all_to_all | solution.py:36
  247.9 25.4 %all-gather.8.cloned.1.call-done = bf16[2048,4224]{1,0:T(8,128)(2,1)} async-done(((bf16[64,4224]{1,0:T(8,128)(2,1)}), bf16[2048,4224]{1,0:T(8,128)(2,1)}) %all-gather.8.cloned.1.call-update) | async-done | bytes 17301520 | tf_op jit(solution)/shard_map/all_gather | solution.py:13
  273.3 5.6 %fusion.25 = f32[256,1408]{1,0:T(8,128)} fusion(bf16[256,2048]{1,0:T(8,128)(2,1)S(1)} %bitcast.41, bf16[2048,4224]{1,0:T(8,128)(2,1)} %all-gather.8.cloned.1.call-done), kind=kOutput, calls=%fused_computation.29 | convolution fusion | flops 1476395008 | bytes 8257536 | tf_op jit(solution)/shard_map/dot_general | solution.py:141
  278.9 8.2 %fusion.33 = bf16[256,2048]{1,0:T(8,128)(2,1)S(1)} fusion(bf16[2048,4224]{1,0:T(8,128)(2,1)} %all-gather.8.cloned.1.call-done, bf16[256,2048]{1,0:T(8,128)(2,1)S(1)} %bitcast.42, f32[256,1408]{1,0:T(8,128)} %fusion.25), kind=kOutput, calls=%fused_computation.34 | convolution fusion | flops 2955476992 | bytes 15073280 | tf_op jit(solution)/shard_map/dot_general | solution.py:146
  287.0 18.4 %all_to_all.16 = bf16[4,64,2048]{2,1,0:T(8,128)(2,1)S(1)} all-to-all(bf16[4,64,2048]{2,1,0:T(8,128)(2,1)S(1)} %bitcast.43), channel_id=1, replica_groups=mesh['grp'=2,'sp'=32,'tp'=4] {'tp'}, dimensions={0} | all-to-all | bytes 2097152 | tf_op jit(solution)/shard_map/all_to_all | solution.py:30
  305.5 0.2 convert_reduce_fusion
  305.6 0.2 multiply_reduce_fusion
  305.8 0.8 multiply_convert_fusion
  (19 shorter events, 0.2 us)
Async XLA Ops:
  6.5 204.1 %copy-start = (bf16[256,2048]{1,0:T(8,128)(2,1)S(1)}, bf16[256,2048]{1,0:T(8,128)(2,1)}, u32[]{:S(2)}) copy-start(bf16[256,2048]{1,0:T(8,128)(2,1)} %param.19) | copy-start | bytes 3145732
  6.6 89.2 %all-gather.4.cloned.1.call-start = ((), (), s32[]{:S(2)}) async-start(), calls=%async_computation.3 | async-start | bytes 4325376 | tf_op jit(solution)/shard_map/all_gather | solution.py:71
  7.3 159.3 %all-gather.6.cloned.1.call-start = ((), (), s32[]{:S(2)}) async-start(), calls=%async_computation.4 | async-start | bytes 4325376 | tf_op jit(solution)/shard_map/all_gather | solution.py:74
  8.1 265.2 %all-gather.8.cloned.1.call-start = ((), (), s32[]{:S(2)}) async-start(), calls=%async_computation.5 | async-start | bytes 17842176 | tf_op jit(solution)/shard_map/all_gather | solution.py:13
  179.5 13.0 %copy-start.1 = (f32[256,4]{0,1:T(4,128)S(1)}, f32[256,4]{0,1:T(4,128)}, u32[]{:S(2)}) copy-start(f32[256,4]{0,1:T(4,128)} %param.18) | copy-start | bytes 12292
  192.5 39.2 %copy-start.2 = (f32[2048]{0:T(1024)S(1)}, f32[2048]{0:T(1024)}, u32[]{:S(2)}) copy-start(f32[2048]{0:T(1024)} %param.20) | copy-start | bytes 24580
  212.1 18.3 %all-to-all-start = ((bf16[4,64,2048]{2,1,0:T(8,128)(2,1)}), bf16[4,64,2048]{2,1,0:T(8,128)(2,1)S(1)}, u32[]{:S(2)}, u32[]{:S(2)}) async-start(bf16[4,64,2048]{2,1,0:T(8,128)(2,1)} %bitcast.10), calls=%async_computation | async-start | bytes 2097152 | tf_op jit(solution)/shard_map/all_to_all | solution.py:30
Sparse Core Ops, SparseCore 0:
  9.2 86.5 all-gather.3
  97.6 68.9 all-gather.5
  168.4 104.8 all-gather.7
where the time goes:
time: 315 us; the launch traced here: 313 us
  waiting for transfers between devices  120 us (38%)
  blocking collectives  85.4 us (27%)
  local copies, waits for them, and re-layouts  55.5 us (18%)
  matrix products  23.6 us (7%)
  between operations  13.3 us (4%)
  other arithmetic  8.64 us (3%)
  starting transfers between devices  3.8 us (1%)
    all_gather x1, blocking collectives, attend(): gate_piece = lax.all_gather(log_gates, 'sp', axis=0, tiled=True)  51.1 us
    all_gather x1, waiting for transfers between devices, attend(): lax.all_gather(values.astype(jnp.float32), 'sp', axis=0, tiled=True)  45 us
    all_gather x1, waiting for transfers between devices, attend(): lax.all_gather(keys.astype(jnp.float32), 'sp', axis=0, tiled=True)  33.5 us
    unnamed x9, local copies, waits for them, and re-layouts  26.9 us
    all_gather x1, waiting for transfers between devices, turned_gather(): result = lax.all_gather(both, axis, axis=0, tiled=True)  25.4 us
    all_to_all x1, blocking collectives, sent_and_summed(): lax.all_to_all(parts, axis, split_axis=0, concat_axis=0, tiled=True)  18.4 us
    all_to_all x1, blocking collectives, sent_to_all(): return lax.all_to_all(copies, axis, split_axis=0, concat_axis=0, tiled=True)  15.9 us
    all_to_all x1, waiting for transfers between devices, sent_and_summed(): lax.all_to_all(parts, axis, split_axis=0, concat_axis=0, tiled=True)  14.6 us
  transfers between devices with their start and end apart: 4, of which 4 were waited for; matrix products, arithmetic and copies ran while one was open for 23% of the time, Pallas kernels for 0%

commit v1 on v0

v1 whole, which is shorter than its diff:
```python
import functools

import jax
import jax.numpy as jnp
from jax import lax
from jax.experimental import pallas as pl
from jax.experimental.pallas import tpu as pltpu
from jax.sharding import PartitionSpec as P

MESH = pl.DeviceIdType.MESH
F32 = jnp.float32
BF16 = jnp.bfloat16
NT_DIMS = (((1,), (1,)), ((), ()))
LANES = 128


def layer_kernel(
    n_sp, n_tp, heads,
    q_ref, kg_ref, v_ref, res_ref, wout_ref, gain_ref, g_ref, u_ref, d_ref,
    out_ref,
    kbuf, vbuf, gbuf, ubuf, dbuf, q4, m_s, l_s, acc, att, pbuf, rsbuf, resv, mixed, nbuf, hid, dsend, drecv, total,
    send_sem, recv_sem, sib_sem, loc_sem, x_send, x_recv,
):
    s = lax.axis_index("sp")
    t = lax.axis_index("tp")
    c = lax.rem(s, 2)
    z = s // 2
    nz = n_sp // 2
    far, near = nz // 2, nz - 1 - nz // 2
    rows, width = q_ref.shape
    head_width = width // heads
    own_rows = rows // n_tp
    drow, ff = g_ref.shape
    model = drow * n_sp

    def chip(offset):
        return lax.rem(z + offset + nz, nz)

    right = chip(1) * 2 + c
    left = chip(-1) * 2 + c
    sibling = s + 1 - 2 * c
    peers = [lax.rem(t + d, n_tp) for d in range(1, n_tp)]
    sources = [lax.rem(t - d + n_tp, n_tp) for d in range(1, n_tp)]

    half = drow // 2
    views = (
        (kbuf, 0, kbuf.shape[1]), (vbuf, 0, vbuf.shape[1]), (gbuf, 0, drow), (ubuf, 0, drow),
        (dbuf, 0, half), (dbuf, half, half),
    )

    def piece(st, slot):
        buf, start, size = views[st]
        return buf.at[slot, pl.ds(start, size)]

    def reach(st):
        return (far, near) if st % 2 == 0 else (near, far)

    def link_copy(st, slot, direction, step):
        return pltpu.make_async_remote_copy(
            src_ref=piece(st, slot), dst_ref=piece(st, slot), send_sem=send_sem.at[st],
            recv_sem=recv_sem.at[st, direction, step - 1],
            device_id={"sp": right if direction == 0 else left}, device_id_type=MESH,
        )

    def sib_copy(st, slot, index):
        return pltpu.make_async_remote_copy(
            src_ref=piece(st, slot), dst_ref=piece(st, slot), send_sem=send_sem.at[st],
            recv_sem=sib_sem.at[st, index], device_id={"sp": sibling}, device_id_type=MESH,
        )

    def send_own(st):
        for direction in (0, 1):
            link_copy(st, s, direction, 1).start()
        sib_copy(st, s, 0).start()

    def arrive(pair, step):
        for st in pair:
            for direction, limit in enumerate(reach(st)):
                @pl.when(step <= limit)
                def _():
                    slot = chip(-step if direction == 0 else step) * 2 + c
                    link_copy(st, slot, direction, step).wait_recv()

                    @pl.when(step < limit)
                    def _():
                        link_copy(st, slot, direction, step + 1).start()

                    sib_copy(st, slot, step + far * direction).start()

    def sib_arrive(pair, step):
        for st in pair:
            for direction, limit in enumerate(reach(st)):
                @pl.when(jnp.logical_and(step >= 1, step <= limit))
                def _():
                    slot = chip(-step if direction == 0 else step) * 2 + 1 - c
                    sib_copy(st, slot, step + far * direction).wait_recv()

            @pl.when(step == 0)
            def _():
                sib_copy(st, sibling, 0).wait_recv()

    def local(src, st, index):
        buf = views[st][0]
        return pltpu.make_async_copy(src, buf.at[s], loc_sem.at[index])

    own_slice = pl.ds(pl.multiple_of(t * own_rows, own_rows), own_rows)
    loads = [local(kg_ref, 0, 0), local(v_ref, 1, 1), local(g_ref, 2, 2), local(u_ref, 3, 3), local(d_ref, 4, 4)]
    loads.append(pltpu.make_async_copy(res_ref.at[own_slice], resv, loc_sem.at[5]))
    for load in loads:
        load.start()

    barrier = pltpu.get_barrier_semaphore()
    for neighbour in (left, right, sibling):
        pl.semaphore_signal(barrier, inc=1, device_id={"sp": neighbour}, device_id_type=MESH)
    for peer in peers:
        pl.semaphore_signal(barrier, inc=1, device_id={"tp": peer}, device_id_type=MESH)
    pl.semaphore_wait(barrier, 3 + n_tp - 1)

    loads[0].wait()
    send_own(0)
    loads[1].wait()
    send_own(1)
    for load in loads[2:]:
        load.wait()

    scaled = q_ref[...].astype(F32) * (head_width ** -0.5)
    lane_head = lax.broadcasted_iota(jnp.int32, (rows, width), 1) // head_width
    for h in range(heads):
        q4[h] = jnp.where(lane_head == h, scaled, 0.0).astype(BF16)
        m_s[h] = jnp.full((rows, LANES), -1e30, F32)
        l_s[h] = jnp.zeros((rows, LANES), F32)
        acc[h] = jnp.zeros((rows, width), F32)

    def wide(x, size):
        return jnp.concatenate([x] * (size // LANES), axis=1) if size >= LANES else x[:, :size]

    def attend(slot, diagonal):
        key = kbuf[slot, 0:rows, :]
        parts = kbuf[slot, rows:rows + 16, :].astype(F32)
        gates = parts[0:heads] + parts[heads:2 * heads] + parts[2 * heads:3 * heads]
        value = vbuf[slot]
        for h in range(heads):
            score = lax.dot_general(q4[h], key, NT_DIMS, preferred_element_type=F32) - gates[h:h + 1, :rows]
            if diagonal:
                at = lax.broadcasted_iota(jnp.int32, (rows, rows), 0)
                col = lax.broadcasted_iota(jnp.int32, (rows, rows), 1)
                score = jnp.where(col <= at, score, -1e30)
            before = m_s[h]
            top = jnp.maximum(before, jnp.max(score, axis=1, keepdims=True))
            weight = jnp.exp(score - wide(top, rows))
            rescale = jnp.exp(before - top)
            lanes = weight[:, 0:LANES]
            for k in range(1, rows // LANES):
                lanes = lanes + weight[:, k * LANES:(k + 1) * LANES]
            l_s[h] = l_s[h] * rescale + lanes
            product = jnp.dot(weight.astype(BF16), value, preferred_element_type=F32)
            acc[h] = acc[h] * wide(rescale, width) + product
            m_s[h] = top

    attend(s, True)

    kv, gu, dn = (0, 1), (2, 3), (4, 5)

    def kv_step(i, _):
        @pl.when(i <= far)
        def _():
            arrive(kv, i)

        @pl.when(i == far - 1)
        def _():
            for st in gu:
                send_own(st)

        j = i - 1
        sib_arrive(kv, j)

        def block(b, _):
            side, core = b // 2, lax.rem(b, 2)
            offset = jnp.where(side == 0, -j, j)
            earlier = jnp.where(side == 0, z - j >= 0, jnp.logical_and(z + j >= nz, j <= near))
            own_chip = jnp.logical_and(side == 0, jnp.logical_and(core == 0, c == 1))
            needed = jnp.where(j == 0, own_chip, earlier)

            @pl.when(needed)
            def _():
                attend(chip(offset) * 2 + core, False)

            return 0

        lax.fori_loop(0, 4, block, 0)
        return 0

    lax.fori_loop(1, far + 2, kv_step, 0)

    arrive(gu, 1)
    merged = jnp.zeros((rows, width), F32)
    for h in range(heads):
        norm = jnp.sum(l_s[h], axis=1, keepdims=True)
        merged = jnp.where(lane_head == h, acc[h] / norm, merged)
    att[...] = merged.astype(BF16)

    tile = min(512, model)

    def project(k, _):
        at = pl.ds(pl.multiple_of(k * tile, tile), tile)
        y = jnp.dot(att[...], wout_ref[:, at], preferred_element_type=F32).astype(BF16)
        pbuf[:, :, at] = y.reshape(n_tp, own_rows, tile)
        return 0

    lax.fori_loop(0, model // tile, project, 0)

    def reduce_copy(d):
        return pltpu.make_async_remote_copy(
            src_ref=pbuf.at[peers[d]], dst_ref=rsbuf.at[t], send_sem=x_send.at[0], recv_sem=x_recv.at[0, d],
            device_id={"tp": peers[d]}, device_id_type=MESH,
        )

    def gather_copy(d):
        return pltpu.make_async_remote_copy(
            src_ref=nbuf.at[t], dst_ref=nbuf.at[t], send_sem=x_send.at[1], recv_sem=x_recv.at[1, d],
            device_id={"tp": peers[d]}, device_id_type=MESH,
        )

    def arrival(buf, sem):
        return pltpu.make_async_copy(buf, buf, sem)

    for d in range(n_tp - 1):
        reduce_copy(d).start()
    arrive(gu, 2)
    arrive(gu, 3)
    for d in range(n_tp - 1):
        arrival(rsbuf.at[sources[d]], x_recv.at[0, d]).wait()
    summed = resv[...].astype(F32) + pbuf[t].astype(F32)
    for d in range(n_tp - 1):
        summed = summed + rsbuf[sources[d]].astype(F32)
    mixed[...] = summed.astype(BF16)
    floats = mixed[...].astype(F32)
    mean = jnp.sum(floats * floats, axis=1, keepdims=True) * (1.0 / model)
    nbuf[t] = (floats * lax.rsqrt(mean + 1e-6) * gain_ref[...]).astype(BF16)
    for d in range(n_tp - 1):
        gather_copy(d).start()

    def gu_step(i, _):
        @pl.when(i == far)
        def _():
            for st in dn:
                send_own(st)

        arrive(gu, i)
        return 0

    lax.fori_loop(4, far + 1, gu_step, 0)

    def gu_sib(i, _):
        sib_arrive(gu, i)
        return 0

    lax.fori_loop(0, far + 1, gu_sib, 0)
    for d in range(n_tp - 1):
        arrival(nbuf.at[sources[d]], x_recv.at[1, d]).wait()

    def ffn(k, _):
        at = pl.ds(pl.multiple_of(k * LANES, LANES), LANES)
        weights = jnp.concatenate(
            [gbuf[:, :, at].reshape(model, LANES), ubuf[:, :, at].reshape(model, LANES)], axis=1
        )
        both = jnp.dot(nbuf[...].reshape(rows, model), weights, preferred_element_type=F32)
        gate, up = both[:, :LANES], both[:, LANES:]
        hid[:, at] = (gate / (1.0 + jnp.exp(-gate)) * up).astype(BF16)

        @pl.when(jnp.logical_and(lax.rem(k, 3) == 2, (k + 1) // 3 <= far))
        def _():
            arrive(dn, (k + 1) // 3)

        return 0

    tiles = ff // LANES
    lax.fori_loop(0, tiles, ffn, 0)
    handled = tiles // 3

    def column_copy(d, at):
        return pltpu.make_async_remote_copy(
            src_ref=dsend.at[at, peers[d]], dst_ref=drecv.at[t, at], send_sem=x_send.at[2],
            recv_sem=x_recv.at[2, d], device_id={"tp": peers[d]}, device_id_type=MESH,
        )

    def down_step(j, _):
        @pl.when(jnp.logical_and(j + 1 > handled, j + 1 <= far))
        def _():
            arrive(dn, j + 1)

        sib_arrive(dn, j)
        back, ahead = chip(-j), chip(j)
        weights = jnp.concatenate(
            [dbuf[pl.ds(at * 2, 2)].reshape(2 * drow, ff) for at in (back, ahead)], axis=0
        )
        y = lax.dot_general(hid[...], weights, NT_DIMS, preferred_element_type=F32).astype(BF16)
        y = y.reshape(n_tp, own_rows, 4 * drow)
        dsend[back] = y[:, :, :2 * drow]
        for d in range(n_tp - 1):
            column_copy(d, back).start()

        @pl.when(jnp.logical_and(j >= 1, j <= near))
        def _():
            dsend[ahead] = y[:, :, 2 * drow:]
            for d in range(n_tp - 1):
                column_copy(d, ahead).start()

        return 0

    lax.fori_loop(0, far + 1, down_step, 0)

    for d in range(n_tp - 1):
        arrival(drecv.at[sources[d]], x_recv.at[2, d]).wait()
    square = jnp.zeros((own_rows, 2 * drow), F32)
    for at in range(nz):
        cols = slice(at * 2 * drow, (at + 1) * 2 * drow)
        down = dsend[at, t].astype(F32)
        for d in range(n_tp - 1):
            down = down + drecv[sources[d], at].astype(F32)
        value = mixed[:, cols].astype(F32) + 0.5 * down
        total[:, cols] = value
        square = square + value * value
    mean = jnp.sum(square, axis=1, keepdims=True) * (1.0 / model)
    out_ref[...] = (total[...] * lax.rsqrt(mean + 1e-6)).astype(BF16)

    for st in range(len(views)):
        buf, start, size = views[st]
        arrival(buf.at[pl.ds(0, 2 * nz - 1), pl.ds(start, size)], send_sem.at[st]).wait()
    arrival(pbuf.at[pl.ds(0, n_tp - 1)], x_send.at[0]).wait()
    arrival(nbuf.at[pl.ds(0, n_tp - 1)], x_send.at[1]).wait()
    arrival(drecv.at[pl.ds(0, n_tp - 1)], x_send.at[2]).wait()


def body(residual, queries, keys, values, log_gates, w_out, norm_gain, w_gate, w_up, w_down):
    n_sp, n_tp = lax.axis_size("sp"), lax.axis_size("tp")
    rows, width = queries.shape
    heads = log_gates.shape[1]
    model = residual.shape[1]
    drow, ff = w_gate.shape
    own_rows = rows // n_tp
    nz = n_sp // 2
    far = nz // 2

    gates = log_gates.T
    high = lax.reduce_precision(gates, 8, 7)
    middle = lax.reduce_precision(gates - high, 8, 7)
    low = gates - high - middle
    extra = jnp.concatenate([high, middle, low, jnp.zeros((16 - 3 * heads, rows), F32)], axis=0).astype(BF16)
    if rows < width:
        extra = jnp.pad(extra, ((0, 0), (0, width - rows)))
    keys_gates = jnp.concatenate([keys, extra], axis=0)

    vmem = pl.BlockSpec(memory_space=pltpu.VMEM)
    hbm = pl.BlockSpec(memory_space=pl.ANY)
    return pl.pallas_call(
        functools.partial(layer_kernel, n_sp, n_tp, heads),
        out_shape=jax.ShapeDtypeStruct((own_rows, model), BF16),
        in_specs=[vmem, hbm, hbm, hbm, vmem, vmem, hbm, hbm, hbm],
        out_specs=vmem,
        scratch_shapes=[
            pltpu.VMEM((n_sp, rows + 16, width), BF16),
            pltpu.VMEM((n_sp, rows, width), BF16),
            pltpu.VMEM((n_sp, drow, ff), BF16),
            pltpu.VMEM((n_sp, drow, ff), BF16),
            pltpu.VMEM((n_sp, drow, ff), BF16),
            pltpu.VMEM((heads, rows, width), BF16),
            pltpu.VMEM((heads, rows, LANES), F32),
            pltpu.VMEM((heads, rows, LANES), F32),
            pltpu.VMEM((heads, rows, width), F32),
            pltpu.VMEM((rows, width), BF16),
            pltpu.VMEM((n_tp, own_rows, model), BF16),
            pltpu.VMEM((n_tp, own_rows, model), BF16),
            pltpu.VMEM((own_rows, model), BF16),
            pltpu.VMEM((own_rows, model), BF16),
            pltpu.VMEM((n_tp, own_rows, model), BF16),
            pltpu.VMEM((rows, ff), BF16),
            pltpu.VMEM((nz, n_tp, own_rows, 2 * drow), BF16),
            pltpu.VMEM((n_tp, nz, own_rows, 2 * drow), BF16),
            pltpu.VMEM((own_rows, model), F32),
            pltpu.SemaphoreType.DMA((6,)),
            pltpu.SemaphoreType.DMA((6, 2, far)),
            pltpu.SemaphoreType.DMA((6, 2 * far + 1)),
            pltpu.SemaphoreType.DMA((6,)),
            pltpu.SemaphoreType.DMA((3,)),
            pltpu.SemaphoreType.DMA((3, n_tp - 1)),
        ],
        compiler_params=pltpu.CompilerParams(
            collective_id=0, has_side_effects=True, vmem_limit_bytes=60 * 1024 * 1024
        ),
    )(queries, keys_gates, values, residual, w_out, norm_gain.reshape(1, -1), w_gate, w_up, w_down.T)


def solution(mesh):
    in_specs = (
        P(("grp", "sp"), None),
        P(("grp", "sp"), "tp"),
        P(("grp", "sp"), "tp"),
        P(("grp", "sp"), "tp"),
        P(("grp", "sp"), "tp"),
        P("tp", None),
        P(),
        P("sp", "tp"),
        P("sp", "tp"),
        P("tp", "sp"),
    )
    out_specs = P(("grp", "sp", "tp"), None)
    return jax.shard_map(body, mesh=mesh, in_specs=in_specs, out_specs=out_specs, check_vma=False)
```

time: 315 us -> 182 us (0.58)
  Pallas kernels: 0 us -> 176 us
  waiting for transfers between devices: 120 us -> 0 us
  blocking collectives: 85.4 us -> 0 us
  local copies, waits for them, and re-layouts: 55.5 us -> 4.47 us
  matrix products: 23.6 us -> 0 us
  between operations: 13.3 us -> 0.01 us
  other arithmetic: 8.64 us -> 0.69 us
  starting transfers between devices: 3.8 us -> 0 us
    pallas_call x0 -> x1, Pallas kernels: none -> 176 us  [body(): pl.pallas_call(functools.partial(layer_kernel, n_sp, n_tp, heads), out_sh...]
    all_gather x3 -> x0, waiting for transfers between devices: 104 us -> none  [the longest x1 45 us: attend(): lax.all_gather(values.astype(jnp.float32), 'sp', axis=0, tiled=True)]
    all_gather x1 -> x0, blocking collectives: 51.1 us -> none  [attend(): gate_piece = lax.all_gather(log_gates, 'sp', axis=0, tiled=True)]
    all_to_all x2 -> x0, blocking collectives: 34.3 us -> none  [the longest x1 18.4 us: sent_and_summed(): lax.all_to_all(parts, axis, split_axis=0, concat_axis=0, tiled=True)]
    reshape x2 -> x0, local copies, waits for them, and re-layouts: 25.8 us -> none  [the longest x1 12.9 us: attend(): key_piece.reshape(block_count, block_rows, head_count, head_width)]
    unnamed x9 -> x1, local copies, waits for them, and re-layouts: 26.9 us -> 1.67 us
    dot_general x5 -> x0, matrix products: 23.6 us -> none  [the longest x1 8.19 us: body(): jnp.dot(rows_part, down_whole, preferred_element_type=jnp.float32)]
    all_to_all x1 -> x0, waiting for transfers between devices: 14.6 us -> none  [sent_and_summed(): lax.all_to_all(parts, axis, split_axis=0, concat_axis=0, tiled=True)]
  transfers between devices with their start and end apart: 4 -> 0, of which waited for: 4 -> 0; matrix products, arithmetic and copies ran while one was open for 23% -> 0% of each run, Pallas kernels for 0% -> 0%
where the time goes in v1:
time: 182 us; the launch traced here: 181 us
  Pallas kernels  176 us (97%)
  local copies, waits for them, and re-layouts  4.47 us (2%)
    pallas_call x1, Pallas kernels, body(): pl.pallas_call(functools.partial(layer_kernel, n_sp, n_tp, heads), out_sh...  176 us

profile of v1, /device:TPU:33, one launch (start us, length us, event | category | flops | bytes accessed | tf_op | source)
XLA Modules:
  0.0 181.4 jit_solution(1791891757637157428)
XLA Ops:
  0.0 0.7 fusion
  0.7 2.8 %concatenate.6.kg_ref = bf16[272,256]{1,0:T(8,128)(2,1)} concatenate(bf16[256,256]{1,0:T(8,128)(2,1)} %param.12, bf16[4,256]{1,0:T(4,128)(2,1)S(1)} %get-tuple-element.7, bf16[4,256]{1,0:T(4,128)(2,1)S(1)} %get-tuple-element.6, bf16[4,256]{1,0:T(4,128)(2,1)S(1)} %get-tuple-element.5, bf16[4,256]{1,0:T(4,128)(2,1)S(1)} %broadcast_in_dim.3), dimensions={0} | concatenate | bytes 278528 | tf_op jit(solution)/shard_map/concatenate | solution.py:352
  3.5 176.3 %shard_map.100 = bf16[64,2048]{1,0:T(8,128)(2,1)} custom-call(bf16[256,256]{1,0:T(8,128)(2,1)} %q_ref.1, bf16[272,256]{1,0:T(8,128)(2,1)} %concatenate.6.kg_ref, bf16[256,256]{1,0:T(8,128)(2,1)} %v_ref.1, bf16[256,2048]{1,0:T(8,128)(2,1)} %res_ref.1, bf16[256,2048]{1,0:T(8,128)(2,1)} %wout_ref.1, f32[1,2048]{1,0:T(1,128)} %bitcast.10, ...), custom_call_target="tpu_custom_call" | custom-call | tf_op jit(solution)/shard_map/pallas_call | solution.py:356
  179.8 1.7 copy.12
  (1 shorter events, 0.0 us)

commit v2 on v1

--- a/solution.py
+++ b/solution.py
@@ -16,10 +16,10 @@
 
 def layer_kernel(
     n_sp, n_tp, heads,
-    q_ref, kg_ref, v_ref, res_ref, wout_ref, gain_ref, g_ref, u_ref, d_ref,
+    q_ref, k_ref, x_ref, v_ref, res_ref, wout_ref, gain_ref, g_ref, u_ref, d_ref,
     out_ref,
-    kbuf, vbuf, gbuf, ubuf, dbuf, q4, m_s, l_s, acc, att, pbuf, rsbuf, resv, mixed, nbuf, hid, dsend, drecv, total,
-    send_sem, recv_sem, sib_sem, loc_sem, x_send, x_recv,
+    kbuf, vbuf, gbuf, ubuf, dbuf, q4, m_s, l_s, acc, att, pbuf, rsbuf, resv, mixed, nbuf, hacc, hid, dsend, drecv, total,
+    send_sem, recv_sem, sib_sem, loc_sem, x_send, x_recv, ack,
 ):
     s = lax.axis_index("sp")
     t = lax.axis_index("tp")
@@ -59,7 +59,7 @@
         return pltpu.make_async_remote_copy(
             src_ref=piece(st, slot), dst_ref=piece(st, slot), send_sem=send_sem.at[st],
             recv_sem=recv_sem.at[st, direction, step - 1],
-            device_id={"sp": right if direction == 0 else left}, device_id_type=MESH,
+            device_id={"sp": jnp.where(direction == 0, right, left)}, device_id_type=MESH,
         )
 
     def sib_copy(st, slot, index):
@@ -73,19 +73,27 @@
             link_copy(st, s, direction, 1).start()
         sib_copy(st, s, 0).start()
 
-    def arrive(pair, step):
-        for st in pair:
-            for direction, limit in enumerate(reach(st)):
-                @pl.when(step <= limit)
-                def _():
-                    slot = chip(-step if direction == 0 else step) * 2 + c
-                    link_copy(st, slot, direction, step).wait_recv()
-
-                    @pl.when(step < limit)
-                    def _():
-                        link_copy(st, slot, direction, step + 1).start()
-
-                    sib_copy(st, slot, step + far * direction).start()
+    def sib_send(st, step):
+        for direction, limit in enumerate(reach(st)):
+            @pl.when(step <= limit)
+            def _():
+                slot = chip(-step if direction == 0 else step) * 2 + c
+                sib_copy(st, slot, step + far * direction).start()
+
+    def arrive(st, step):
+        for direction, limit in enumerate(reach(st)):
+            @pl.when(step <= limit)
+            def _():
+                slot = chip(-step if direction == 0 else step) * 2 + c
+                link_copy(st, slot, direction, step).wait_recv()
+
+                @pl.when(step < limit)
+                def _():
+                    link_copy(st, slot, direction, step + 1).start()
+
+    def arrive_both(st, step):
+        arrive(st, step)
+        sib_send(st, step)
 
     def sib_arrive(pair, step):
         for st in pair:
@@ -99,28 +107,59 @@
             def _():
                 sib_copy(st, sibling, 0).wait_recv()
 
-    def local(src, st, index):
-        buf = views[st][0]
-        return pltpu.make_async_copy(src, buf.at[s], loc_sem.at[index])
+    def local(src, dst, index):
+        return pltpu.make_async_copy(src, dst, loc_sem.at[index])
 
     own_slice = pl.ds(pl.multiple_of(t * own_rows, own_rows), own_rows)
-    loads = [local(kg_ref, 0, 0), local(v_ref, 1, 1), local(g_ref, 2, 2), local(u_ref, 3, 3), local(d_ref, 4, 4)]
-    loads.append(pltpu.make_async_copy(res_ref.at[own_slice], resv, loc_sem.at[5]))
+    loads = [
+        local(k_ref, kbuf.at[s, pl.ds(0, rows)], 0), local(x_ref, kbuf.at[s, pl.ds(rows, 16)], 1),
+        local(v_ref, vbuf.at[s], 2), local(g_ref, gbuf.at[s], 3), local(u_ref, ubuf.at[s], 4),
+        local(d_ref, dbuf.at[s], 5), local(res_ref.at[own_slice], resv, 6),
+    ]
     for load in loads:
         load.start()
 
+    lower = [z > 0, z == nz - 1, c == 1] + [peer < t for peer in peers]
+    axis = ["sp", "sp", "sp"] + ["tp"] * (n_tp - 1)
+    partner = [left, right, sibling] + peers
+    theirs = [1, 0, 2] + [2 + n_tp - d for d in range(1, n_tp)]
     barrier = pltpu.get_barrier_semaphore()
-    for neighbour in (left, right, sibling):
-        pl.semaphore_signal(barrier, inc=1, device_id={"sp": neighbour}, device_id_type=MESH)
-    for peer in peers:
-        pl.semaphore_signal(barrier, inc=1, device_id={"tp": peer}, device_id_type=MESH)
-    pl.semaphore_wait(barrier, 3 + n_tp - 1)
-
+    for k in range(2 + n_tp):
+        @pl.when(lower[k])
+        def _():
+            pl.semaphore_signal(barrier, inc=1, device_id={axis[k]: partner[k]}, device_id_type=MESH)
+
+    higher = sum(jnp.where(low, 0, 1) for low in lower)
+
+    @pl.when(higher > 0)
+    def _():
+        pl.semaphore_wait(barrier, higher)
+
+    for k in range(2 + n_tp):
+        @pl.when(jnp.logical_not(lower[k]))
+        def _():
+            pl.semaphore_signal(
+                ack.at[theirs[k]], inc=1, device_id={axis[k]: partner[k]}, device_id_type=MESH
+            )
+
+    def ready(k):
+        @pl.when(lower[k])
+        def _():
+            pl.semaphore_wait(ack.at[k], 1)
+
+    last = z == nz - 1
     loads[0].wait()
-    send_own(0)
     loads[1].wait()
-    send_own(1)
-    for load in loads[2:]:
+    loads[2].wait()
+    for turn in (0, 1):
+        for direction in (0, 1):
+            @pl.when(last == (direction != turn))
+            def _():
+                ready(1 - direction)
+                link_copy(0, s, direction, 1).start()
+                link_copy(1, s, direction, 1).start()
+
+    for load in loads[3:]:
         load.wait()
 
     scaled = q_ref[...].astype(F32) * (head_width ** -0.5)
@@ -160,39 +199,61 @@
     attend(s, True)
 
     kv, gu, dn = (0, 1), (2, 3), (4, 5)
+    hold = min(3, far - 1)
 
     def kv_step(i, _):
-        @pl.when(i <= far)
-        def _():
-            arrive(kv, i)
-
-        @pl.when(i == far - 1)
-        def _():
-            for st in gu:
-                send_own(st)
-
-        j = i - 1
-        sib_arrive(kv, j)
-
-        def block(b, _):
-            side, core = b // 2, lax.rem(b, 2)
-            offset = jnp.where(side == 0, -j, j)
-            earlier = jnp.where(side == 0, z - j >= 0, jnp.logical_and(z + j >= nz, j <= near))
-            own_chip = jnp.logical_and(side == 0, jnp.logical_and(core == 0, c == 1))
-            needed = jnp.where(j == 0, own_chip, earlier)
-
-            @pl.when(needed)
-            def _():
-                attend(chip(offset) * 2 + core, False)
-
-            return 0
-
-        lax.fori_loop(0, 4, block, 0)
+        for half, st in enumerate(kv):
+            @pl.when(i <= far)
+            def _():
+                arrive(st, i)
+
+                @pl.when(i == hold)
+                def _():
+                    if half == 0:
+                        ready(2)
+                    sib_copy(st, s, 0).start()
+                    for step in range(1, hold):
+                        sib_send(st, step)
+
+                @pl.when(i >= hold)
+                def _():
+                    sib_send(st, i)
+
+            if half == 1:
+                @pl.when(i == far - 1)
+                def _():
+                    for own in gu:
+                        send_own(own)
+
+            late = 2 * (i - far // 2 - 1) + half
+
+            @pl.when(jnp.logical_and(late >= 0, late <= far))
+            def _():
+                sib_arrive(kv, late)
+
+            def block(b, _):
+                own = b == 0
+                j = jnp.where(own, i - 1, late)
+                core = jnp.where(own, c, 1 - c)
+                back = jnp.where(own, half == 0, b == 1)
+                offset = jnp.where(back, -j, j)
+                earlier = jnp.where(back, z - j >= 0, jnp.logical_and(z + j >= nz, j <= near))
+                at_home = jnp.logical_and(jnp.logical_not(own), jnp.logical_and(back, c == 1))
+                needed = jnp.where(j == 0, at_home, earlier)
+
+                @pl.when(jnp.logical_and(needed, jnp.logical_and(j >= 0, j <= far)))
+                def _():
+                    attend(chip(offset) * 2 + core, False)
+
+                return 0
+
+            lax.fori_loop(0, 3, block, 0)
         return 0
 
     lax.fori_loop(1, far + 2, kv_step, 0)
 
-    arrive(gu, 1)
+    for st in gu:
+        arrive_both(st, 1)
     merged = jnp.zeros((rows, width), F32)
     for h in range(heads):
         norm = jnp.sum(l_s[h], axis=1, keepdims=True)
@@ -224,10 +285,13 @@
     def arrival(buf, sem):
         return pltpu.make_async_copy(buf, buf, sem)
 
-    for d in range(n_tp - 1):
+    arrive_both(gu[0], 2)
+    for d in range(n_tp - 1):
+        ready(3 + d)
         reduce_copy(d).start()
-    arrive(gu, 2)
-    arrive(gu, 3)
+    arrive_both(gu[1], 2)
+    for st in gu:
+        arrive_both(st, 3)
     for d in range(n_tp - 1):
         arrival(rsbuf.at[sources[d]], x_recv.at[0, d]).wait()
     summed = resv[...].astype(F32) + pbuf[t].astype(F32)
@@ -241,42 +305,62 @@
         gather_copy(d).start()
 
     def gu_step(i, _):
-        @pl.when(i == far)
-        def _():
-            for st in dn:
-                send_own(st)
-
-        arrive(gu, i)
+        for st in gu:
+            arrive_both(st, i)
         return 0
 
-    lax.fori_loop(4, far + 1, gu_step, 0)
-
-    def gu_sib(i, _):
-        sib_arrive(gu, i)
-        return 0
-
-    lax.fori_loop(0, far + 1, gu_sib, 0)
+    lax.fori_loop(4, far - 2, gu_step, 0)
+
+    tiles = ff // LANES
+    chip_rows = 2 * drow
+
+    def accumulate(offsets, first, final):
+        for j in sorted({abs(o) for o in offsets}):
+            sib_arrive(gu, j)
+        chips = [chip(o) for o in offsets]
+        left_side = jnp.concatenate(
+            [nbuf[:, :, pl.ds(pl.multiple_of(at * chip_rows, chip_rows), chip_rows)] for at in chips], axis=2
+        ).reshape(rows, len(chips) * chip_rows)
+
+        def one(k, _):
+            at = pl.ds(pl.multiple_of(k * LANES, LANES), LANES)
+            sides = [
+                jnp.concatenate(
+                    [buf[pl.ds(2 * chosen, 2), :, at].reshape(chip_rows, LANES) for chosen in chips], axis=0
+                )
+                for buf in (gbuf, ubuf)
+            ]
+            both = jnp.dot(left_side, jnp.concatenate(sides, axis=1), preferred_element_type=F32)
+            if not first:
+                both = both + hacc[k]
+            if final:
+                gate, up = both[:, :LANES], both[:, LANES:]
+                hid[:, at] = (gate / (1.0 + jnp.exp(-gate)) * up).astype(BF16)
+            else:
+                hacc[k] = both
+            return 0
+
+        lax.fori_loop(0, tiles, one, 0)
+
+    def around(*distances):
+        return [o for j in distances for o in (-j, j)]
+
+    arrive_both(gu[0], far - 2)
     for d in range(n_tp - 1):
         arrival(nbuf.at[sources[d]], x_recv.at[1, d]).wait()
-
-    def ffn(k, _):
-        at = pl.ds(pl.multiple_of(k * LANES, LANES), LANES)
-        weights = jnp.concatenate(
-            [gbuf[:, :, at].reshape(model, LANES), ubuf[:, :, at].reshape(model, LANES)], axis=1
-        )
-        both = jnp.dot(nbuf[...].reshape(rows, model), weights, preferred_element_type=F32)
-        gate, up = both[:, :LANES], both[:, LANES:]
-        hid[:, at] = (gate / (1.0 + jnp.exp(-gate)) * up).astype(BF16)
-
-        @pl.when(jnp.logical_and(lax.rem(k, 3) == 2, (k + 1) // 3 <= far))
-        def _():
-            arrive(dn, (k + 1) // 3)
-
-        return 0
-
-    tiles = ff // LANES
-    lax.fori_loop(0, tiles, ffn, 0)
-    handled = tiles // 3
+    accumulate([0] + around(1), True, False)
+    arrive_both(gu[1], far - 2)
+    accumulate(around(2, 3), False, False)
+    arrive_both(gu[0], far - 1)
+    accumulate(around(*range(4, far - 2)), False, False)
+    arrive_both(gu[1], far - 1)
+    for st in dn:
+        send_own(st)
+    accumulate(around(far - 2), False, False)
+    arrive_both(gu[0], far)
+    accumulate(around(far - 1), False, False)
+    arrive_both(gu[1], far)
+    accumulate([-far], False, True)
 
     def column_copy(d, at):
         return pltpu.make_async_remote_copy(
@@ -285,9 +369,10 @@
         )
 
     def down_step(j, _):
-        @pl.when(jnp.logical_and(j + 1 > handled, j + 1 <= far))
+        @pl.when(j + 1 <= far)
         def _():
-            arrive(dn, j + 1)
+            for st in dn:
+                arrive_both(st, j + 1)
 
         sib_arrive(dn, j)
         back, ahead = chip(-j), chip(j)
@@ -347,16 +432,12 @@
     middle = lax.reduce_precision(gates - high, 8, 7)
     low = gates - high - middle
     extra = jnp.concatenate([high, middle, low, jnp.zeros((16 - 3 * heads, rows), F32)], axis=0).astype(BF16)
-    if rows < width:
-        extra = jnp.pad(extra, ((0, 0), (0, width - rows)))
-    keys_gates = jnp.concatenate([keys, extra], axis=0)
-
     vmem = pl.BlockSpec(memory_space=pltpu.VMEM)
     hbm = pl.BlockSpec(memory_space=pl.ANY)
     return pl.pallas_call(
         functools.partial(layer_kernel, n_sp, n_tp, heads),
         out_shape=jax.ShapeDtypeStruct((own_rows, model), BF16),
-        in_specs=[vmem, hbm, hbm, hbm, vmem, vmem, hbm, hbm, hbm],
+        in_specs=[vmem, hbm, hbm, hbm, hbm, vmem, vmem, hbm, hbm, hbm],
         out_specs=vmem,
         scratch_shapes=[
             pltpu.VMEM((n_sp, rows + 16, width), BF16),
@@ -374,6 +455,7 @@
             pltpu.VMEM((own_rows, model), BF16),
             pltpu.VMEM((own_rows, model), BF16),
             pltpu.VMEM((n_tp, own_rows, model), BF16),
+            pltpu.VMEM((ff // LANES, rows, 2 * LANES), F32),
             pltpu.VMEM((rows, ff), BF16),
             pltpu.VMEM((nz, n_tp, own_rows, 2 * drow), BF16),
             pltpu.VMEM((n_tp, nz, own_rows, 2 * drow), BF16),
@@ -381,14 +463,15 @@
             pltpu.SemaphoreType.DMA((6,)),
             pltpu.SemaphoreType.DMA((6, 2, far)),
             pltpu.SemaphoreType.DMA((6, 2 * far + 1)),
-            pltpu.SemaphoreType.DMA((6,)),
+            pltpu.SemaphoreType.DMA((7,)),
             pltpu.SemaphoreType.DMA((3,)),
             pltpu.SemaphoreType.DMA((3, n_tp - 1)),
+            pltpu.SemaphoreType.REGULAR((2 + n_tp,)),
         ],
         compiler_params=pltpu.CompilerParams(
             collective_id=0, has_side_effects=True, vmem_limit_bytes=60 * 1024 * 1024
         ),
-    )(queries, keys_gates, values, residual, w_out, norm_gain.reshape(1, -1), w_gate, w_up, w_down.T)
+    )(queries, keys, extra, values, residual, w_out, norm_gain.reshape(1, -1), w_gate, w_up, w_down.T)
 
 
 def solution(mesh):

time: 182 us -> 181 us (level)
  local copies, waits for them, and re-layouts: 4.47 us -> 2.36 us
  Pallas kernels: 176 us -> 178 us
    concatenate x1, local copies, waits for them, and re-layouts: 2.79 us -> 0.08 us  [body(): jnp.concatenate([high, middle, low, jnp.zeros((16 - 3 * heads, rows), F32...]
where the time goes in v2:
time: 181 us
  Pallas kernels  178 us (98%)
  local copies, waits for them, and re-layouts  2.36 us (1%)
    pallas_call x1, Pallas kernels, body(): pl.pallas_call(functools.partial(layer_kernel, n_sp, n_tp, heads), out_sh...  178 us

profile of v2, /device:TPU:33, one launch (start us, length us, event | category | flops | bytes accessed | tf_op | source)
XLA Modules:
  0.0 181.1 jit_solution(893734601340303483)
XLA Ops:
  0.0 0.0 copy-start
  0.0 0.1 pad.3.clone
  0.1 0.6 copy-done
  0.7 0.7 maximum_maximum_fusion.x_ref
  1.4 178.0 %shard_map.100 = bf16[64,2048]{1,0:T(8,128)(2,1)} custom-call(bf16[256,256]{1,0:T(8,128)(2,1)} %q_ref.1, bf16[256,256]{1,0:T(8,128)(2,1)} %k_ref.1, bf16[16,256]{1,0:T(8,128)(2,1)} %maximum_maximum_fusion.x_ref, bf16[256,256]{1,0:T(8,128)(2,1)} %v_ref.1, bf16[256,2048]{1,0:T(8,128)(2,1)} %res_ref.1, bf16[256,2048]{1,0:T(8,128)(2,1)} %wout_ref.1, ...), custom_call_target="tpu_custom_call" | custom-call | tf_op jit(solution)/shard_map/pallas_call | solution.py:437
  179.4 1.7 copy.12
  (2 shorter events, 0.0 us)
Async XLA Ops:
  0.0 0.7 copy-start

commit v3 on v2

v3 whole, which is shorter than its diff:
```python
import functools

import jax
import jax.numpy as jnp
from jax import lax
from jax.experimental import pallas as pl
from jax.experimental.pallas import tpu as pltpu
from jax.sharding import PartitionSpec as P

MESH = pl.DeviceIdType.MESH
F32 = jnp.float32
BF16 = jnp.bfloat16
NT_DIMS = (((1,), (1,)), ((), ()))
LANES = 128


def layer_kernel(
    n_sp, n_tp, heads,
    q_ref, k_ref, x_ref, v_ref, res_ref, wout_ref, gain_ref, g_ref, u_ref, d_ref,
    out_ref,
    kbuf, vbuf, gbuf, ubuf, dbuf, q4, m_s, l_s, acc, att, pbuf, rsbuf, resv, mixed, nbuf, hacc, hid, dsend, drecv, total,
    qfar, ofar, osend, sfar, ssend,
    send_sem, recv_sem, sib_sem, loc_sem, x_send, x_recv, ack, kv_send, kv_sib, pair_sem,
):
    s = lax.axis_index("sp")
    t = lax.axis_index("tp")
    c = lax.rem(s, 2)
    z = s // 2
    nz = n_sp // 2
    far, near = nz // 2, nz - 1 - nz // 2
    rows, width = q_ref.shape
    head_width = width // heads
    own_rows = rows // n_tp
    drow, ff = g_ref.shape
    model = drow * n_sp

    def chip(offset):
        return lax.rem(z + offset + nz, nz)

    right = chip(1) * 2 + c
    left = chip(-1) * 2 + c
    sibling = s + 1 - 2 * c
    pair = chip(far) * 2 + c
    upper = z >= far
    peers = [lax.rem(t + d, n_tp) for d in range(1, n_tp)]
    sources = [lax.rem(t - d + n_tp, n_tp) for d in range(1, n_tp)]

    half = drow // 2
    views = (
        (kbuf, 0, kbuf.shape[1]), (vbuf, 0, vbuf.shape[1]), (gbuf, 0, drow), (ubuf, 0, drow),
        (dbuf, 0, half), (dbuf, half, half),
    )

    def piece(st, slot):
        buf, start, size = views[st]
        return buf.at[slot, pl.ds(start, size)]

    reaches = ((near, 0), (near, 0), (near - 1, far + 1), (near, far), (near, far), (near, far))
    ways = nz

    def reach(st):
        return reaches[st]

    def link_copy(st, slot, direction, step):
        return pltpu.make_async_remote_copy(
            src_ref=piece(st, slot), dst_ref=piece(st, slot),
            send_sem=kv_send.at[st, step - 1] if st < 2 else send_sem.at[st],
            recv_sem=recv_sem.at[st, direction, step - 1],
            device_id={"sp": right if direction == 0 else left}, device_id_type=MESH,
        )

    def sib_copy(st, slot, index):
        return pltpu.make_async_remote_copy(
            src_ref=piece(st, slot), dst_ref=piece(st, slot),
            send_sem=kv_sib.at[st, index] if st < 2 else send_sem.at[st],
            recv_sem=sib_sem.at[st, index], device_id={"sp": sibling}, device_id_type=MESH,
        )

    def usable(st, direction, step):
        fits = jnp.logical_and(step >= 1, step <= reach(st)[direction])
        return jnp.logical_and(fits, z - step >= 0) if st < 2 else fits

    def source(direction, step):
        return chip(-step if direction == 0 else step)

    def send_own(st, direction):
        link_copy(st, s, direction, 1).start()

    def arrive(st, direction, step):
        @pl.when(usable(st, direction, step))
        def _():
            slot = source(direction, step) * 2 + c
            link_copy(st, slot, direction, step).wait_recv()
            onward = step < reach(st)[direction]

            @pl.when(jnp.logical_and(onward, z < nz - 1) if st < 2 else onward)
            def _():
                link_copy(st, slot, direction, step + 1).start()

            sib_copy(st, slot, step + ways * direction).start()

    def sib_arrive(pair_of, step):
        for st in pair_of:
            for direction in (0, 1):
                @pl.when(usable(st, direction, step))
                def _():
                    slot = source(direction, step) * 2 + 1 - c
                    sib_copy(st, slot, step + ways * direction).wait_recv()

            @pl.when(step == 0)
            def _():
                sib_copy(st, sibling, 0).wait_recv()

    def local(src, dst, index):
        return pltpu.make_async_copy(src, dst, loc_sem.at[index])

    own_slice = pl.ds(pl.multiple_of(t * own_rows, own_rows), own_rows)
    loads = [
        local(k_ref, kbuf.at[s, pl.ds(0, rows)], 0), local(x_ref, kbuf.at[s, pl.ds(rows, 16)], 1),
        local(v_ref, vbuf.at[s], 2), local(g_ref, gbuf.at[s], 3), local(u_ref, ubuf.at[s], 4),
        local(d_ref, dbuf.at[s], 5), local(res_ref.at[own_slice], resv, 6),
    ]
    for load in loads:
        load.start()

    lower = [z == 0, z < nz - 1, c == 1, jnp.logical_not(upper)] + [peer < t for peer in peers]
    axis = ["sp", "sp", "sp", "sp"] + ["tp"] * (n_tp - 1)
    partner = [left, right, sibling, pair] + peers
    theirs = [1, 0, 2, 3] + [3 + n_tp - d for d in range(1, n_tp)]
    barrier = pltpu.get_barrier_semaphore()
    for k in range(3 + n_tp):
        @pl.when(lower[k])
        def _():
            pl.semaphore_signal(barrier, inc=1, device_id={axis[k]: partner[k]}, device_id_type=MESH)

    higher = sum(jnp.where(low, 0, 1) for low in lower)

    @pl.when(higher > 0)
    def _():
        pl.semaphore_wait(barrier, higher)

    for k in range(3 + n_tp):
        @pl.when(jnp.logical_not(lower[k]))
        def _():
            pl.semaphore_signal(
                ack.at[theirs[k]], inc=1, device_id={axis[k]: partner[k]}, device_id_type=MESH
            )

    def ready(k):
        @pl.when(lower[k])
        def _():
            pl.semaphore_wait(ack.at[k], 1)

    kv, gu, dn = (0, 1), (2, 3), (4, 5)
    edge = jnp.logical_or(z == 0, z == nz - 1)
    for load in loads[:3]:
        load.wait()
    ready(1)

    @pl.when(z < nz - 1)
    def _():
        for st in kv:
            send_own(st, 0)

    query_copy = pltpu.make_async_remote_copy(
        src_ref=q_ref, dst_ref=qfar, send_sem=pair_sem.at[0], recv_sem=pair_sem.at[1],
        device_id={"sp": pair}, device_id_type=MESH,
    )

    @pl.when(upper)
    def _():
        query_copy.start()

    for load in loads[3:]:
        load.wait()

    @pl.when(edge)
    def _():
        for st in gu:
            send_own(st, 0)

    ready(2)
    for st in kv:
        sib_copy(st, s, 0).start()
    ready(0)
    for st in gu:
        send_own(st, 1)
    for st in gu + dn:
        sib_copy(st, s, 0).start()

    lane_head = lax.broadcasted_iota(jnp.int32, (rows, width), 1) // head_width

    def prepare(which, ref):
        scaled = ref[...].astype(F32) * (head_width ** -0.5)
        for h in range(heads):
            q4[which, h] = jnp.where(lane_head == h, scaled, 0.0).astype(BF16)
            m_s[which, h] = jnp.full((rows, LANES), -1e30, F32)
            l_s[which, h] = jnp.zeros((rows, LANES), F32)
            acc[which, h] = jnp.zeros((rows, width), F32)

    prepare(0, q_ref)

    def wide(x, size):
        return jnp.concatenate([x] * (size // LANES), axis=1) if size >= LANES else x[:, :size]

    def attend(which, slot, diagonal):
        key = kbuf[slot, 0:rows, :]
        parts = kbuf[slot, rows:rows + 16, :].astype(F32)
        gates = parts[0:heads] + parts[heads:2 * heads] + parts[2 * heads:3 * heads]
        value = vbuf[slot]
        for h in range(heads):
            score = lax.dot_general(q4[which, h], key, NT_DIMS, preferred_element_type=F32) - gates[h:h + 1, :rows]
            if diagonal:
                at = lax.broadcasted_iota(jnp.int32, (rows, rows), 0)
                col = lax.broadcasted_iota(jnp.int32, (rows, rows), 1)
                score = jnp.where(col <= at, score, -1e30)
            before = m_s[which, h]
            top = jnp.maximum(before, jnp.max(score, axis=1, keepdims=True))
            weight = jnp.exp(score - wide(top, rows))
            rescale = jnp.exp(before - top)
            lanes = weight[:, 0:LANES]
            for k in range(1, rows // LANES):
                lanes = lanes + weight[:, k * LANES:(k + 1) * LANES]
            l_s[which, h] = l_s[which, h] * rescale + lanes
            product = jnp.dot(weight.astype(BF16), value, preferred_element_type=F32)
            acc[which, h] = acc[which, h] * wide(rescale, width) + product
            m_s[which, h] = top

    attend(0, s, True)

    ahead_from = near - 1

    def kv_step(i, _):
        for half, st in enumerate(kv):
            arrive(st, 0, i)
            if half == 1:
                @pl.when(jnp.logical_and(jnp.logical_not(edge), i == jnp.minimum(z, near - 1)))
                def _():
                    for own in gu:
                        send_own(own, 0)

                @pl.when(lax.rem(i, 2) == 0)
                def _():
                    for own in gu:
                        arrive(own, 1, jnp.where(i <= near, i // 2, 0))

                @pl.when(i <= far)
                def _():
                    sib_arrive(kv, i - 1)

                @pl.when(jnp.logical_and(i == ahead_from - 1, jnp.logical_not(upper)))
                def _():
                    query_copy.wait_recv()
                    prepare(1, qfar)

            turn = 2 * (i - ahead_from) + half

            def block(b, _):
                which = jnp.where(b == 0, 0, 1)
                j = jnp.where(b == 0, i - 1, turn)
                core = jnp.where(b == 0, c if half == 0 else 1 - c, b - 1)
                fits = jnp.logical_and(jnp.logical_and(j >= 0, j <= near), z - j >= 0)
                own = jnp.logical_or(j > 0, jnp.logical_and(half == 1, c == 1))
                needed = jnp.logical_and(fits, jnp.where(b == 0, own, jnp.logical_not(upper)))

                @pl.when(needed)
                def _():
                    attend(which, chip(-j) * 2 + core, False)

                return 0

            lax.fori_loop(0, 3, block, 0)
        return 0

    lax.fori_loop(1, far + 2, kv_step, 0)

    early = near // 2

    def gu_step(k):
        for st in gu:
            arrive(st, 0, k)
            arrive(st, 1, k + early)

    def merge(which):
        merged = jnp.zeros((rows, width), F32)
        for h in range(heads):
            norm = jnp.sum(l_s[which, h], axis=1, keepdims=True)
            merged = jnp.where(lane_head == h, acc[which, h] / norm, merged)
        return merged

    def far_copy(k):
        return pltpu.make_async_remote_copy(
            src_ref=(osend, ssend)[k], dst_ref=(ofar, sfar)[k], send_sem=pair_sem.at[2 + k],
            recv_sem=pair_sem.at[4 + k], device_id={"sp": pair}, device_id_type=MESH,
        )

    lane = lax.broadcasted_iota(jnp.int32, (rows, LANES), 1)

    @pl.when(jnp.logical_not(upper))
    def _():
        osend[...] = merge(1).astype(BF16)
        stats = jnp.zeros((rows, LANES), F32)
        for h in range(heads):
            stats = jnp.where(lane == h, m_s[1, h], stats)
            stats = jnp.where(lane == heads + h, jnp.sum(l_s[1, h], axis=1, keepdims=True), stats)
        ssend[...] = stats.T[0:2 * heads, :]

    for direction_step in (1,):
        gu_step(direction_step)

    @pl.when(jnp.logical_not(upper))
    def _():
        ready(3)
        for k in (0, 1):
            far_copy(k).start()
        att[...] = merge(0).astype(BF16)

    gu_step(2)

    @pl.when(upper)
    def _():
        for k in (0, 1):
            far_copy(k).wait_recv()
        stats = jnp.concatenate([sfar[...], jnp.zeros((LANES - 2 * heads, rows), F32)], axis=0).T
        other = ofar[...].astype(F32)
        merged = jnp.zeros((rows, width), F32)
        for h in range(heads):
            mine, theirs_max = m_s[0, h][:, 0:1], stats[:, h:h + 1]
            top = jnp.maximum(mine, theirs_max)
            mine_scale = jnp.exp(mine - top)
            theirs_sum = stats[:, heads + h:heads + h + 1] * jnp.exp(theirs_max - top)
            norm = jnp.sum(l_s[0, h], axis=1, keepdims=True) * mine_scale + theirs_sum
            merged = jnp.where(lane_head == h, (acc[0, h] * mine_scale + other * theirs_sum) / norm, merged)
        att[...] = merged.astype(BF16)

    tile = min(512, model)

    def project(k, _):
        at = pl.ds(pl.multiple_of(k * tile, tile), tile)
        y = jnp.dot(att[...], wout_ref[:, at], preferred_element_type=F32).astype(BF16)
        pbuf[:, :, at] = y.reshape(n_tp, own_rows, tile)
        return 0

    lax.fori_loop(0, model // tile, project, 0)

    def reduce_copy(d):
        return pltpu.make_async_remote_copy(
            src_ref=pbuf.at[peers[d]], dst_ref=rsbuf.at[t], send_sem=x_send.at[0], recv_sem=x_recv.at[0, d],
            device_id={"tp": peers[d]}, device_id_type=MESH,
        )

    def gather_copy(d):
        return pltpu.make_async_remote_copy(
            src_ref=nbuf.at[t], dst_ref=nbuf.at[t], send_sem=x_send.at[1], recv_sem=x_recv.at[1, d],
            device_id={"tp": peers[d]}, device_id_type=MESH,
        )

    def arrival(buf, sem):
        return pltpu.make_async_copy(buf, buf, sem)

    gu_step(3)
    for d in range(n_tp - 1):
        ready(4 + d)
        reduce_copy(d).start()
    for k in range(4, near - 1):
        gu_step(k)
    for d in range(n_tp - 1):
        arrival(rsbuf.at[sources[d]], x_recv.at[0, d]).wait()
    summed = resv[...].astype(F32) + pbuf[t].astype(F32)
    for d in range(n_tp - 1):
        summed = summed + rsbuf[sources[d]].astype(F32)
    mixed[...] = summed.astype(BF16)
    floats = mixed[...].astype(F32)
    mean = jnp.sum(floats * floats, axis=1, keepdims=True) * (1.0 / model)
    nbuf[t] = (floats * lax.rsqrt(mean + 1e-6) * gain_ref[...]).astype(BF16)
    for d in range(n_tp - 1):
        gather_copy(d).start()

    gu_step(near - 1)
    for st in dn:
        send_own(st, 1)
        send_own(st, 0)
    gu_step(near)

    def gu_sib(i, _):
        sib_arrive(gu, i)
        return 0

    lax.fori_loop(0, far + 2, gu_sib, 0)
    for d in range(n_tp - 1):
        arrival(nbuf.at[sources[d]], x_recv.at[1, d]).wait()

    tiles = ff // LANES
    chip_rows = 2 * drow

    def accumulate(offsets, first, final):
        chips = [chip(o) for o in offsets]
        left_side = jnp.concatenate(
            [nbuf[:, :, pl.ds(pl.multiple_of(at * chip_rows, chip_rows), chip_rows)] for at in chips], axis=2
        ).reshape(rows, len(chips) * chip_rows)

        def one(k, _):
            at = pl.ds(pl.multiple_of(k * LANES, LANES), LANES)
            sides = [
                jnp.concatenate(
                    [buf[pl.ds(2 * chosen, 2), :, at].reshape(chip_rows, LANES) for chosen in chips], axis=0
                )
                for buf in (gbuf, ubuf)
            ]
            both = jnp.dot(left_side, jnp.concatenate(sides, axis=1), preferred_element_type=F32)
            if not first:
                both = both + hacc[k]
            if final:
                gate, up = both[:, :LANES], both[:, LANES:]
                hid[:, at] = (gate / (1.0 + jnp.exp(-gate)) * up).astype(BF16)
            else:
                hacc[k] = both
            return 0

        lax.fori_loop(0, tiles, one, 0)

    def dn_step(k):
        for st in dn:
            for direction in (0, 1):
                arrive(st, direction, k)

    offsets = [0] + [o for j in range(1, far) for o in (-j, j)] + [far]
    group = -(-len(offsets) // 4)
    for k in range(4):
        accumulate(offsets[k * group:(k + 1) * group], k == 0, k == 3)
        dn_step(k + 1)

    def column_copy(d, at):
        return pltpu.make_async_remote_copy(
            src_ref=dsend.at[at, peers[d]], dst_ref=drecv.at[t, at], send_sem=x_send.at[2],
            recv_sem=x_recv.at[2, d], device_id={"tp": peers[d]}, device_id_type=MESH,
        )

    def down_step(j, _):
        @pl.when(jnp.logical_and(j + 2 > 4, j + 2 <= far))
        def _():
            dn_step(j + 2)

        sib_arrive(dn, j)
        back, ahead = chip(j), chip(-j)
        weights = jnp.concatenate(
            [dbuf[pl.ds(at * 2, 2)].reshape(2 * drow, ff) for at in (back, ahead)], axis=0
        )
        y = lax.dot_general(hid[...], weights, NT_DIMS, preferred_element_type=F32).astype(BF16)
        y = y.reshape(n_tp, own_rows, 4 * drow)
        dsend[back] = y[:, :, :2 * drow]
        for d in range(n_tp - 1):
            column_copy(d, back).start()

        @pl.when(jnp.logical_and(j >= 1, j <= near))
        def _():
            dsend[ahead] = y[:, :, 2 * drow:]
            for d in range(n_tp - 1):
                column_copy(d, ahead).start()

        return 0

    lax.fori_loop(0, far + 1, down_step, 0)

    for d in range(n_tp - 1):
        arrival(drecv.at[sources[d]], x_recv.at[2, d]).wait()
    square = jnp.zeros((own_rows, 2 * drow), F32)
    for at in range(nz):
        cols = slice(at * 2 * drow, (at + 1) * 2 * drow)
        down = dsend[at, t].astype(F32)
        for d in range(n_tp - 1):
            down = down + drecv[sources[d], at].astype(F32)
        value = mixed[:, cols].astype(F32) + 0.5 * down
        total[:, cols] = value
        square = square + value * value
    mean = jnp.sum(square, axis=1, keepdims=True) * (1.0 / model)
    out_ref[...] = (total[...] * lax.rsqrt(mean + 1e-6)).astype(BF16)

    for st in kv:
        for k in range(near):
            @pl.when(jnp.logical_and(z < nz - 1, z >= k))
            def _():
                link_copy(st, s, 0, k + 1).wait_send()

        for k in range(near + 1):
            @pl.when(z >= k)
            def _():
                sib_copy(st, s, k).wait_send()

    @pl.when(upper)
    def _():
        query_copy.wait_send()

    @pl.when(jnp.logical_not(upper))
    def _():
        for k in (0, 1):
            far_copy(k).wait_send()

    for st in gu + dn:
        buf, start, size = views[st]
        arrival(buf.at[pl.ds(0, 2 * nz - 1), pl.ds(start, size)], send_sem.at[st]).wait()
    arrival(pbuf.at[pl.ds(0, n_tp - 1)], x_send.at[0]).wait()
    arrival(nbuf.at[pl.ds(0, n_tp - 1)], x_send.at[1]).wait()
    arrival(drecv.at[pl.ds(0, n_tp - 1)], x_send.at[2]).wait()


def body(residual, queries, keys, values, log_gates, w_out, norm_gain, w_gate, w_up, w_down):
    n_sp, n_tp = lax.axis_size("sp"), lax.axis_size("tp")
    rows, width = queries.shape
    heads = log_gates.shape[1]
    model = residual.shape[1]
    drow, ff = w_gate.shape
    own_rows = rows // n_tp
    nz = n_sp // 2
    far = nz // 2

    gates = log_gates.T
    high = lax.reduce_precision(gates, 8, 7)
    middle = lax.reduce_precision(gates - high, 8, 7)
    low = gates - high - middle
    extra = jnp.concatenate([high, middle, low, jnp.zeros((16 - 3 * heads, rows), F32)], axis=0).astype(BF16)
    vmem = pl.BlockSpec(memory_space=pltpu.VMEM)
    hbm = pl.BlockSpec(memory_space=pl.ANY)
    return pl.pallas_call(
        functools.partial(layer_kernel, n_sp, n_tp, heads),
        out_shape=jax.ShapeDtypeStruct((own_rows, model), BF16),
        in_specs=[vmem, hbm, hbm, hbm, hbm, vmem, vmem, hbm, hbm, hbm],
        out_specs=vmem,
        scratch_shapes=[
            pltpu.VMEM((n_sp, rows + 16, width), BF16),
            pltpu.VMEM((n_sp, rows, width), BF16),
            pltpu.VMEM((n_sp, drow, ff), BF16),
            pltpu.VMEM((n_sp, drow, ff), BF16),
            pltpu.VMEM((n_sp, drow, ff), BF16),
            pltpu.VMEM((2, heads, rows, width), BF16),
            pltpu.VMEM((2, heads, rows, LANES), F32),
            pltpu.VMEM((2, heads, rows, LANES), F32),
            pltpu.VMEM((2, heads, rows, width), F32),
            pltpu.VMEM((rows, width), BF16),
            pltpu.VMEM((n_tp, own_rows, model), BF16),
            pltpu.VMEM((n_tp, own_rows, model), BF16),
            pltpu.VMEM((own_rows, model), BF16),
            pltpu.VMEM((own_rows, model), BF16),
            pltpu.VMEM((n_tp, own_rows, model), BF16),
            pltpu.VMEM((ff // LANES, rows, 2 * LANES), F32),
            pltpu.VMEM((rows, ff), BF16),
            pltpu.VMEM((nz, n_tp, own_rows, 2 * drow), BF16),
            pltpu.VMEM((n_tp, nz, own_rows, 2 * drow), BF16),
            pltpu.VMEM((own_rows, model), F32),
            pltpu.VMEM((rows, width), BF16),
            pltpu.VMEM((rows, width), BF16),
            pltpu.VMEM((rows, width), BF16),
            pltpu.VMEM((2 * heads, rows), F32),
            pltpu.VMEM((2 * heads, rows), F32),
            pltpu.SemaphoreType.DMA((6,)),
            pltpu.SemaphoreType.DMA((6, 2, far + 1)),
            pltpu.SemaphoreType.DMA((6, nz + far + 2)),
            pltpu.SemaphoreType.DMA((7,)),
            pltpu.SemaphoreType.DMA((3,)),
            pltpu.SemaphoreType.DMA((3, n_tp - 1)),
            pltpu.SemaphoreType.REGULAR((3 + n_tp,)),
            pltpu.SemaphoreType.DMA((2, far)),
            pltpu.SemaphoreType.DMA((2, far)),
            pltpu.SemaphoreType.DMA((6,)),
        ],
        compiler_params=pltpu.CompilerParams(
            collective_id=0, has_side_effects=True, vmem_limit_bytes=60 * 1024 * 1024
        ),
    )(queries, keys, extra, values, residual, w_out, norm_gain.reshape(1, -1), w_gate, w_up, w_down.T)


def solution(mesh):
    in_specs = (
        P(("grp", "sp"), None),
        P(("grp", "sp"), "tp"),
        P(("grp", "sp"), "tp"),
        P(("grp", "sp"), "tp"),
        P(("grp", "sp"), "tp"),
        P("tp", None),
        P(),
        P("sp", "tp"),
        P("sp", "tp"),
        P("tp", "sp"),
    )
    out_specs = P(("grp", "sp", "tp"), None)
    return jax.shard_map(body, mesh=mesh, in_specs=in_specs, out_specs=out_specs, check_vma=False)
```

time: 181 us -> 181 us (level)
  no operation moved by 1% of the time
where the time goes in v3:
time: 181 us; the launch traced here: 180 us
  Pallas kernels  177 us (98%)
  local copies, waits for them, and re-layouts  2.36 us (1%)
    pallas_call x1, Pallas kernels, body(): pl.pallas_call(functools.partial(layer_kernel, n_sp, n_tp, heads), out_sh...  177 us

profile of v3, /device:TPU:33, one launch (start us, length us, event | category | flops | bytes accessed | tf_op | source)
XLA Modules:
  0.0 180.4 jit_solution(926112325730015174)
XLA Ops:
  0.0 0.0 copy-start
  0.0 0.1 pad.3.clone
  0.1 0.6 copy-done
  0.7 0.7 maximum_maximum_fusion.x_ref
  1.4 177.4 %shard_map.100 = bf16[64,2048]{1,0:T(8,128)(2,1)} custom-call(bf16[256,256]{1,0:T(8,128)(2,1)} %q_ref.1, bf16[256,256]{1,0:T(8,128)(2,1)} %k_ref.1, bf16[16,256]{1,0:T(8,128)(2,1)} %maximum_maximum_fusion.x_ref, bf16[256,256]{1,0:T(8,128)(2,1)} %v_ref.1, bf16[256,2048]{1,0:T(8,128)(2,1)} %res_ref.1, bf16[256,2048]{1,0:T(8,128)(2,1)} %wout_ref.1, ...), custom_call_target="tpu_custom_call" | custom-call | tf_op jit(solution)/shard_map/pallas_call | solution.py:524
  178.8 1.7 copy.12
  (2 shorter events, 0.0 us)
Async XLA Ops:
  0.0 0.7 copy-start

commit v4 on v3

--- a/solution.py
+++ b/solution.py
@@ -55,7 +55,10 @@
         buf, start, size = views[st]
         return buf.at[slot, pl.ds(start, size)]
 
-    reaches = ((near, 0), (near, 0), (near - 1, far + 1), (near, far), (near, far), (near, far))
+    right_hops = nz // 4 + 1
+    left_hops = nz - 1 - right_hops
+    both_ways = (right_hops, left_hops)
+    reaches = ((near, 0), (near, 0), (right_hops - 1, left_hops + 1), both_ways, both_ways, both_ways)
     ways = nz
 
     def reach(st):
@@ -239,10 +242,8 @@
                     for own in gu:
                         send_own(own, 0)
 
-                @pl.when(lax.rem(i, 2) == 0)
-                def _():
-                    for own in gu:
-                        arrive(own, 1, jnp.where(i <= near, i // 2, 0))
+                for own in gu:
+                    arrive(own, 1, jnp.where(i <= near, i, 0))
 
                 @pl.when(i <= far)
                 def _():
@@ -274,12 +275,35 @@
 
     lax.fori_loop(1, far + 2, kv_step, 0)
 
-    early = near // 2
-
-    def gu_step(k):
+    lag = jnp.minimum(near + 3, jnp.maximum(near, near + 5 - z))
+    down_from = 2 * (left_hops + 2)
+
+    def pump(h, _):
         for st in gu:
-            arrive(st, 0, k)
-            arrive(st, 1, k + early)
+            arrive(st, 1, jnp.where(lax.rem(h, 2) == 0, h // 2, 0))
+
+        @pl.when(h == 2 * left_hops)
+        def _():
+            for st in dn:
+                send_own(st, 1)
+
+        for st in dn:
+            arrive(st, 1, h - down_from + 1)
+        turn = jnp.where(lax.rem(h, 2) == 0, h // 2 - lag, 0)
+        for st in gu:
+            arrive(st, 0, turn)
+
+        @pl.when(turn == right_hops - 1)
+        def _():
+            for st in dn:
+                send_own(st, 0)
+
+        for st in dn:
+            arrive(st, 0, h - 2 * (lag + right_hops + 1) + 1)
+        return 0
+
+    def pumps(first, last):
+        lax.fori_loop(first, last, pump, 0)
 
     def merge(which):
         merged = jnp.zeros((rows, width), F32)
@@ -305,17 +329,15 @@
             stats = jnp.where(lane == heads + h, jnp.sum(l_s[1, h], axis=1, keepdims=True), stats)
         ssend[...] = stats.T[0:2 * heads, :]
 
-    for direction_step in (1,):
-        gu_step(direction_step)
-
     @pl.when(jnp.logical_not(upper))
     def _():
+        att[...] = merge(0).astype(BF16)
         ready(3)
         for k in (0, 1):
             far_copy(k).start()
-        att[...] = merge(0).astype(BF16)
-
-    gu_step(2)
+
+    start = 2 * (near + 1)
+    pumps(start, start + 3)
 
     @pl.when(upper)
     def _():
@@ -358,12 +380,11 @@
     def arrival(buf, sem):
         return pltpu.make_async_copy(buf, buf, sem)
 
-    gu_step(3)
+    pumps(start + 3, start + 4)
     for d in range(n_tp - 1):
         ready(4 + d)
         reduce_copy(d).start()
-    for k in range(4, near - 1):
-        gu_step(k)
+    pumps(start + 4, down_from + 1)
     for d in range(n_tp - 1):
         arrival(rsbuf.at[sources[d]], x_recv.at[0, d]).wait()
     summed = resv[...].astype(F32) + pbuf[t].astype(F32)
@@ -376,17 +397,19 @@
     for d in range(n_tp - 1):
         gather_copy(d).start()
 
-    gu_step(near - 1)
-    for st in dn:
-        send_own(st, 1)
-        send_own(st, 0)
-    gu_step(near)
-
-    def gu_sib(i, _):
-        sib_arrive(gu, i)
-        return 0
-
-    lax.fori_loop(0, far + 2, gu_sib, 0)
+    fill = down_from + 5
+    pumps(down_from + 1, fill)
+
+    def sib_offset(streams, offset):
+        for st in streams:
+            if offset == 0:
+                index = 0
+            elif offset > 0:
+                index = offset + ways
+            else:
+                index = -offset if -offset <= reach(st)[0] else nz + offset + ways
+            sib_copy(st, chip(offset) * 2 + 1 - c, index).wait_recv()
+
     for d in range(n_tp - 1):
         arrival(nbuf.at[sources[d]], x_recv.at[1, d]).wait()
 
@@ -394,6 +417,8 @@
     chip_rows = 2 * drow
 
     def accumulate(offsets, first, final):
+        for offset in offsets:
+            sib_offset(gu, offset)
         chips = [chip(o) for o in offsets]
         left_side = jnp.concatenate(
             [nbuf[:, :, pl.ds(pl.multiple_of(at * chip_rows, chip_rows), chip_rows)] for at in chips], axis=2
@@ -419,16 +444,11 @@
 
         lax.fori_loop(0, tiles, one, 0)
 
-    def dn_step(k):
-        for st in dn:
-            for direction in (0, 1):
-                arrive(st, direction, k)
-
-    offsets = [0] + [o for j in range(1, far) for o in (-j, j)] + [far]
-    group = -(-len(offsets) // 4)
+    spread = [0] + list(range(1, left_hops + 1)) + [-j for j in range(1, right_hops + 1)]
+    group = -(-len(spread) // 4)
     for k in range(4):
-        accumulate(offsets[k * group:(k + 1) * group], k == 0, k == 3)
-        dn_step(k + 1)
+        accumulate(spread[k * group:(k + 1) * group], k == 0, k == 3)
+        pumps(fill + k, fill + k + 1)
 
     def column_copy(d, at):
         return pltpu.make_async_remote_copy(
@@ -436,31 +456,31 @@
             recv_sem=x_recv.at[2, d], device_id={"tp": peers[d]}, device_id_type=MESH,
         )
 
-    def down_step(j, _):
-        @pl.when(jnp.logical_and(j + 2 > 4, j + 2 <= far))
-        def _():
-            dn_step(j + 2)
-
-        sib_arrive(dn, j)
-        back, ahead = chip(j), chip(-j)
-        weights = jnp.concatenate(
-            [dbuf[pl.ds(at * 2, 2)].reshape(2 * drow, ff) for at in (back, ahead)], axis=0
-        )
+    def down(offsets):
+        for offset in offsets:
+            sib_offset(dn, offset)
+        chips = [chip(offset) for offset in offsets]
+        weights = jnp.concatenate([dbuf[pl.ds(at * 2, 2)].reshape(2 * drow, ff) for at in chips], axis=0)
         y = lax.dot_general(hid[...], weights, NT_DIMS, preferred_element_type=F32).astype(BF16)
         y = y.reshape(n_tp, own_rows, 4 * drow)
-        dsend[back] = y[:, :, :2 * drow]
-        for d in range(n_tp - 1):
-            column_copy(d, back).start()
-
-        @pl.when(jnp.logical_and(j >= 1, j <= near))
-        def _():
-            dsend[ahead] = y[:, :, 2 * drow:]
+        for k, at in enumerate(chips):
+            dsend[at] = y[:, :, 2 * drow * k:2 * drow * (k + 1)]
+        for at in chips:
             for d in range(n_tp - 1):
-                column_copy(d, ahead).start()
-
-        return 0
-
-    lax.fori_loop(0, far + 1, down_step, 0)
+                column_copy(d, at).start()
+
+    backs, fronts = [-j for j in range(1, right_hops + 1)], list(range(1, left_hops + 1))
+    sequence = [0] + fronts[:len(fronts) - right_hops]
+    for ahead, back in zip(fronts[len(fronts) - right_hops:], backs):
+        sequence += [ahead, back]
+    last = 2 * (near + 3 + right_hops + 1) + right_hops
+    at_pump = fill + 4
+    while sequence:
+        down(sequence[:2])
+        sequence = sequence[2:]
+        if len(sequence) <= 2 * (last - at_pump) and at_pump < last:
+            pumps(at_pump, at_pump + 1)
+            at_pump += 1
 
     for d in range(n_tp - 1):
         arrival(drecv.at[sources[d]], x_recv.at[2, d]).wait()
@@ -553,8 +573,8 @@
             pltpu.VMEM((2 * heads, rows), F32),
             pltpu.VMEM((2 * heads, rows), F32),
             pltpu.SemaphoreType.DMA((6,)),
-            pltpu.SemaphoreType.DMA((6, 2, far + 1)),
-            pltpu.SemaphoreType.DMA((6, nz + far + 2)),
+            pltpu.SemaphoreType.DMA((6, 2, nz)),
+            pltpu.SemaphoreType.DMA((6, 2 * nz)),
             pltpu.SemaphoreType.DMA((7,)),
             pltpu.SemaphoreType.DMA((3,)),
             pltpu.SemaphoreType.DMA((3, n_tp - 1)),

time: 181 us -> 263 us (1.45)
  the two profiles are of different devices: /device:TPU:33 before, /device:TPU:548 now
where the time goes in v4:
time: 263 us
  Pallas kernels  260 us (99%)
    pallas_call x1, Pallas kernels, body(): pl.pallas_call(functools.partial(layer_kernel, n_sp, n_tp, heads), out_sh...  260 us

profile of v4, /device:TPU:548, one launch (start us, length us, event | category | flops | bytes accessed | tf_op | source)
XLA Modules:
  0.0 262.7 jit_solution(24081583176391609)
XLA Ops:
  0.0 0.0 copy-start
  0.0 0.1 pad.3.clone
  0.1 0.6 copy-done
  0.7 0.7 maximum_maximum_fusion.x_ref
  1.4 259.6 %shard_map.100 = bf16[64,2048]{1,0:T(8,128)(2,1)} custom-call(bf16[256,256]{1,0:T(8,128)(2,1)} %q_ref.1, bf16[256,256]{1,0:T(8,128)(2,1)} %k_ref.1, bf16[16,256]{1,0:T(8,128)(2,1)} %maximum_maximum_fusion.x_ref, bf16[256,256]{1,0:T(8,128)(2,1)} %v_ref.1, bf16[256,2048]{1,0:T(8,128)(2,1)} %res_ref.1, bf16[256,2048]{1,0:T(8,128)(2,1)} %wout_ref.1, ...), custom_call_target="tpu_custom_call" | custom-call | tf_op jit(solution)/shard_map/pallas_call | solution.py:544
  261.0 1.7 copy.12
  (2 shorter events, 0.0 us)
Async XLA Ops:
  0.0 0.7 copy-start

commit v5 on v3

--- a/solution.py
+++ b/solution.py
@@ -19,7 +19,7 @@
     q_ref, k_ref, x_ref, v_ref, res_ref, wout_ref, gain_ref, g_ref, u_ref, d_ref,
     out_ref,
     kbuf, vbuf, gbuf, ubuf, dbuf, q4, m_s, l_s, acc, att, pbuf, rsbuf, resv, mixed, nbuf, hacc, hid, dsend, drecv, total,
-    qfar, ofar, osend, sfar, ssend,
+    qmid, qfar, omid, ofar, osend, smid, sfar, ssend,
     send_sem, recv_sem, sib_sem, loc_sem, x_send, x_recv, ack, kv_send, kv_sib, pair_sem,
 ):
     s = lax.axis_index("sp")
@@ -40,8 +40,11 @@
     right = chip(1) * 2 + c
     left = chip(-1) * 2 + c
     sibling = s + 1 - 2 * c
-    pair = chip(far) * 2 + c
+    quarter = nz // 4
+    behind, beyond = chip(-quarter) * 2 + c, chip(quarter) * 2 + c
     upper = z >= far
+    passes_query = jnp.logical_and(z >= quarter, z < nz - quarter)
+    passes_output = jnp.logical_not(passes_query)
     peers = [lax.rem(t + d, n_tp) for d in range(1, n_tp)]
     sources = [lax.rem(t - d + n_tp, n_tp) for d in range(1, n_tp)]
 
@@ -123,12 +126,13 @@
     for load in loads:
         load.start()
 
-    lower = [z == 0, z < nz - 1, c == 1, jnp.logical_not(upper)] + [peer < t for peer in peers]
-    axis = ["sp", "sp", "sp", "sp"] + ["tp"] * (n_tp - 1)
-    partner = [left, right, sibling, pair] + peers
-    theirs = [1, 0, 2, 3] + [3 + n_tp - d for d in range(1, n_tp)]
+    lower = [z == 0, z < nz - 1, c == 1, z < quarter, z < nz - quarter]
+    lower += [peer < t for peer in peers]
+    axis = ["sp"] * 5 + ["tp"] * (n_tp - 1)
+    partner = [left, right, sibling, behind, beyond] + peers
+    theirs = [1, 0, 2, None, 3] + [4 + n_tp - d for d in range(1, n_tp)]
     barrier = pltpu.get_barrier_semaphore()
-    for k in range(3 + n_tp):
+    for k in range(4 + n_tp):
         @pl.when(lower[k])
         def _():
             pl.semaphore_signal(barrier, inc=1, device_id={axis[k]: partner[k]}, device_id_type=MESH)
@@ -139,7 +143,10 @@
     def _():
         pl.semaphore_wait(barrier, higher)
 
-    for k in range(3 + n_tp):
+    for k in range(4 + n_tp):
+        if theirs[k] is None:
+            continue
+
         @pl.when(jnp.logical_not(lower[k]))
         def _():
             pl.semaphore_signal(
@@ -162,10 +169,16 @@
         for st in kv:
             send_own(st, 0)
 
-    query_copy = pltpu.make_async_remote_copy(
-        src_ref=q_ref, dst_ref=qfar, send_sem=pair_sem.at[0], recv_sem=pair_sem.at[1],
-        device_id={"sp": pair}, device_id_type=MESH,
-    )
+    def back_copy(src, dst, send, receive):
+        return pltpu.make_async_remote_copy(
+            src_ref=src, dst_ref=dst, send_sem=pair_sem.at[send], recv_sem=pair_sem.at[receive],
+            device_id={"sp": behind}, device_id_type=MESH,
+        )
+
+    query_copy = back_copy(q_ref, qmid, 0, 2)
+    query_relay = back_copy(qmid, qfar, 1, 3)
+    outputs = [back_copy(osend, omid, 4, 8), back_copy(ssend, smid, 5, 9)]
+    output_relays = [back_copy(omid, ofar, 6, 10), back_copy(smid, sfar, 7, 11)]
 
     @pl.when(upper)
     def _():
@@ -248,9 +261,14 @@
                 def _():
                     sib_arrive(kv, i - 1)
 
+                @pl.when(jnp.logical_and(i == 2, passes_query))
+                def _():
+                    query_copy.wait_recv()
+                    query_relay.start()
+
                 @pl.when(jnp.logical_and(i == ahead_from - 1, jnp.logical_not(upper)))
                 def _():
-                    query_copy.wait_recv()
+                    query_relay.wait_recv()
                     prepare(1, qfar)
 
             turn = 2 * (i - ahead_from) + half
@@ -288,12 +306,6 @@
             merged = jnp.where(lane_head == h, acc[which, h] / norm, merged)
         return merged
 
-    def far_copy(k):
-        return pltpu.make_async_remote_copy(
-            src_ref=(osend, ssend)[k], dst_ref=(ofar, sfar)[k], send_sem=pair_sem.at[2 + k],
-            recv_sem=pair_sem.at[4 + k], device_id={"sp": pair}, device_id_type=MESH,
-        )
-
     lane = lax.broadcasted_iota(jnp.int32, (rows, LANES), 1)
 
     @pl.when(jnp.logical_not(upper))
@@ -305,22 +317,28 @@
             stats = jnp.where(lane == heads + h, jnp.sum(l_s[1, h], axis=1, keepdims=True), stats)
         ssend[...] = stats.T[0:2 * heads, :]
 
-    for direction_step in (1,):
-        gu_step(direction_step)
-
     @pl.when(jnp.logical_not(upper))
     def _():
+        att[...] = merge(0).astype(BF16)
         ready(3)
-        for k in (0, 1):
-            far_copy(k).start()
-        att[...] = merge(0).astype(BF16)
+        for copy in outputs:
+            copy.start()
+
+    gu_step(1)
+
+    @pl.when(passes_output)
+    def _():
+        for copy in outputs:
+            copy.wait_recv()
+        for copy in output_relays:
+            copy.start()
 
     gu_step(2)
 
     @pl.when(upper)
     def _():
-        for k in (0, 1):
-            far_copy(k).wait_recv()
+        for copy in output_relays:
+            copy.wait_recv()
         stats = jnp.concatenate([sfar[...], jnp.zeros((LANES - 2 * heads, rows), F32)], axis=0).T
         other = ofar[...].astype(F32)
         merged = jnp.zeros((rows, width), F32)
@@ -360,7 +378,7 @@
 
     gu_step(3)
     for d in range(n_tp - 1):
-        ready(4 + d)
+        ready(5 + d)
         reduce_copy(d).start()
     for k in range(4, near - 1):
         gu_step(k)
@@ -491,10 +509,19 @@
     def _():
         query_copy.wait_send()
 
+    @pl.when(passes_query)
+    def _():
+        query_relay.wait_send()
+
     @pl.when(jnp.logical_not(upper))
     def _():
-        for k in (0, 1):
-            far_copy(k).wait_send()
+        for copy in outputs:
+            copy.wait_send()
+
+    @pl.when(passes_output)
+    def _():
+        for copy in output_relays:
+            copy.wait_send()
 
     for st in gu + dn:
         buf, start, size = views[st]
@@ -547,21 +574,18 @@
             pltpu.VMEM((nz, n_tp, own_rows, 2 * drow), BF16),
             pltpu.VMEM((n_tp, nz, own_rows, 2 * drow), BF16),
             pltpu.VMEM((own_rows, model), F32),
-            pltpu.VMEM((rows, width), BF16),
-            pltpu.VMEM((rows, width), BF16),
-            pltpu.VMEM((rows, width), BF16),
-            pltpu.VMEM((2 * heads, rows), F32),
-            pltpu.VMEM((2 * heads, rows), F32),
+            *[pltpu.VMEM((rows, width), BF16) for _ in range(5)],
+            *[pltpu.VMEM((2 * heads, rows), F32) for _ in range(3)],
             pltpu.SemaphoreType.DMA((6,)),
             pltpu.SemaphoreType.DMA((6, 2, far + 1)),
             pltpu.SemaphoreType.DMA((6, nz + far + 2)),
             pltpu.SemaphoreType.DMA((7,)),
             pltpu.SemaphoreType.DMA((3,)),
             pltpu.SemaphoreType.DMA((3, n_tp - 1)),
-            pltpu.SemaphoreType.REGULAR((3 + n_tp,)),
+            pltpu.SemaphoreType.REGULAR((4 + n_tp,)),
             pltpu.SemaphoreType.DMA((2, far)),
             pltpu.SemaphoreType.DMA((2, far)),
-            pltpu.SemaphoreType.DMA((6,)),
+            pltpu.SemaphoreType.DMA((12,)),
         ],
         compiler_params=pltpu.CompilerParams(
             collective_id=0, has_side_effects=True, vmem_limit_bytes=60 * 1024 * 1024

time: 181 us -> 182 us (level)
  Pallas kernels: 177 us -> 179 us
where the time goes in v5:
time: 182 us
  Pallas kernels  179 us (98%)
  local copies, waits for them, and re-layouts  2.36 us (1%)
    pallas_call x1, Pallas kernels, body(): pl.pallas_call(functools.partial(layer_kernel, n_sp, n_tp, heads), out_sh...  179 us

profile of v5, /device:TPU:33, one launch (start us, length us, event | category | flops | bytes accessed | tf_op | source)
XLA Modules:
  0.0 182.2 jit_solution(8192389392674639533)
XLA Ops:
  0.0 0.0 copy-start
  0.0 0.1 pad.3.clone
  0.1 0.6 copy-done
  0.7 0.7 maximum_maximum_fusion.x_ref
  1.4 179.2 %shard_map.100 = bf16[64,2048]{1,0:T(8,128)(2,1)} custom-call(bf16[256,256]{1,0:T(8,128)(2,1)} %q_ref.1, bf16[256,256]{1,0:T(8,128)(2,1)} %k_ref.1, bf16[16,256]{1,0:T(8,128)(2,1)} %maximum_maximum_fusion.x_ref, bf16[256,256]{1,0:T(8,128)(2,1)} %v_ref.1, bf16[256,2048]{1,0:T(8,128)(2,1)} %res_ref.1, bf16[256,2048]{1,0:T(8,128)(2,1)} %wout_ref.1, ...), custom_call_target="tpu_custom_call" | custom-call | tf_op jit(solution)/shard_map/pallas_call | solution.py:551
  180.5 1.7 copy.12
  (2 shorter events, 0.0 us)
Async XLA Ops:
  0.0 0.7 copy-start

commit v6 on v5

--- a/solution.py
+++ b/solution.py
@@ -241,7 +241,7 @@
 
     attend(0, s, True)
 
-    ahead_from = near - 1
+    ahead_from = near - 2
 
     def kv_step(i, _):
         for half, st in enumerate(kv):
@@ -252,10 +252,8 @@
                     for own in gu:
                         send_own(own, 0)
 
-                @pl.when(lax.rem(i, 2) == 0)
-                def _():
-                    for own in gu:
-                        arrive(own, 1, jnp.where(i <= near, i // 2, 0))
+                for own in gu:
+                    arrive(own, 1, jnp.where(i >= far - 2, i - far + 4, jnp.where(i == far - 4, 1, 0)) * (i <= near))
 
                 @pl.when(i <= far)
                 def _():
@@ -290,9 +288,9 @@
             lax.fori_loop(0, 3, block, 0)
         return 0
 
-    lax.fori_loop(1, far + 2, kv_step, 0)
-
-    early = near // 2
+    lax.fori_loop(1, far + 1, kv_step, 0)
+
+    early = 3
 
     def gu_step(k):
         for st in gu:
@@ -376,10 +374,13 @@
     def arrival(buf, sem):
         return pltpu.make_async_copy(buf, buf, sem)
 
-    gu_step(3)
+    arrive(gu[0], 0, 3)
+    arrive(gu[0], 1, 3 + early)
     for d in range(n_tp - 1):
         ready(5 + d)
         reduce_copy(d).start()
+    arrive(gu[1], 0, 3)
+    arrive(gu[1], 1, 3 + early)
     for k in range(4, near - 1):
         gu_step(k)
     for d in range(n_tp - 1):
@@ -399,6 +400,13 @@
         send_own(st, 1)
         send_own(st, 0)
     gu_step(near)
+
+    def dn_step(k):
+        for st in dn:
+            for direction in (0, 1):
+                arrive(st, direction, k)
+
+    dn_step(1)
 
     def gu_sib(i, _):
         sib_arrive(gu, i)
@@ -437,16 +445,11 @@
 
         lax.fori_loop(0, tiles, one, 0)
 
-    def dn_step(k):
-        for st in dn:
-            for direction in (0, 1):
-                arrive(st, direction, k)
-
     offsets = [0] + [o for j in range(1, far) for o in (-j, j)] + [far]
     group = -(-len(offsets) // 4)
     for k in range(4):
         accumulate(offsets[k * group:(k + 1) * group], k == 0, k == 3)
-        dn_step(k + 1)
+        dn_step(k + 2)
 
     def column_copy(d, at):
         return pltpu.make_async_remote_copy(
@@ -455,9 +458,9 @@
         )
 
     def down_step(j, _):
-        @pl.when(jnp.logical_and(j + 2 > 4, j + 2 <= far))
+        @pl.when(jnp.logical_and(lax.rem(j, 3) == 0, 6 + j // 3 <= far))
         def _():
-            dn_step(j + 2)
+            dn_step(6 + j // 3)
 
         sib_arrive(dn, j)
         back, ahead = chip(j), chip(-j)

time: 182 us -> 186 us (1.022)
  Pallas kernels: 179 us -> 182 us
    pallas_call x1, Pallas kernels: 179 us -> 182 us  [body(): pl.pallas_call(functools.partial(layer_kernel, n_sp, n_tp, heads), out_sh...]
where the time goes in v6:
time: 186 us; the launch traced here: 185 us
  Pallas kernels  182 us (98%)
  local copies, waits for them, and re-layouts  2.36 us (1%)
    pallas_call x1, Pallas kernels, body(): pl.pallas_call(functools.partial(layer_kernel, n_sp, n_tp, heads), out_sh...  182 us

profile of v6, /device:TPU:33, one launch (start us, length us, event | category | flops | bytes accessed | tf_op | source)
XLA Modules:
  0.0 184.9 jit_solution(10916515335978542329)
XLA Ops:
  0.0 0.0 copy-start
  0.0 0.1 pad.3.clone
  0.1 0.6 copy-done
  0.7 0.7 maximum_maximum_fusion.x_ref
  1.4 181.9 %shard_map.100 = bf16[64,2048]{1,0:T(8,128)(2,1)} custom-call(bf16[256,256]{1,0:T(8,128)(2,1)} %q_ref.1, bf16[256,256]{1,0:T(8,128)(2,1)} %k_ref.1, bf16[16,256]{1,0:T(8,128)(2,1)} %maximum_maximum_fusion.x_ref, bf16[256,256]{1,0:T(8,128)(2,1)} %v_ref.1, bf16[256,2048]{1,0:T(8,128)(2,1)} %res_ref.1, bf16[256,2048]{1,0:T(8,128)(2,1)} %wout_ref.1, ...), custom_call_target="tpu_custom_call" | custom-call | tf_op jit(solution)/shard_map/pallas_call | solution.py:554
  183.2 1.7 copy.12
  (2 shorter events, 0.0 us)
Async XLA Ops:
  0.0 0.7 copy-start

commit v7 on v3

--- a/solution.py
+++ b/solution.py
@@ -55,7 +55,10 @@
         buf, start, size = views[st]
         return buf.at[slot, pl.ds(start, size)]
 
-    reaches = ((near, 0), (near, 0), (near - 1, far + 1), (near, far), (near, far), (near, far))
+    right_hops = near - 1
+    left_hops = nz - 1 - right_hops
+    both_ways = (right_hops, left_hops)
+    reaches = ((near, 0), (near, 0), (right_hops - 1, left_hops + 1), both_ways, both_ways, both_ways)
     ways = nz
 
     def reach(st):
@@ -239,10 +242,8 @@
                     for own in gu:
                         send_own(own, 0)
 
-                @pl.when(lax.rem(i, 2) == 0)
-                def _():
-                    for own in gu:
-                        arrive(own, 1, jnp.where(i <= near, i // 2, 0))
+                for own in gu:
+                    arrive(own, 1, jnp.where(i >= 5, i - 2, jnp.where(i == 4, 0, i - 1)) * (i <= near))
 
                 @pl.when(i <= far)
                 def _():
@@ -274,7 +275,7 @@
 
     lax.fori_loop(1, far + 2, kv_step, 0)
 
-    early = near // 2
+    early = near - 2
 
     def gu_step(k):
         for st in gu:
@@ -362,8 +363,11 @@
     for d in range(n_tp - 1):
         ready(4 + d)
         reduce_copy(d).start()
-    for k in range(4, near - 1):
+    for k in range(4, right_hops):
         gu_step(k)
+    for st in dn:
+        send_own(st, 1)
+        send_own(st, 0)
     for d in range(n_tp - 1):
         arrival(rsbuf.at[sources[d]], x_recv.at[0, d]).wait()
     summed = resv[...].astype(F32) + pbuf[t].astype(F32)
@@ -376,17 +380,20 @@
     for d in range(n_tp - 1):
         gather_copy(d).start()
 
-    gu_step(near - 1)
-    for st in dn:
-        send_own(st, 1)
-        send_own(st, 0)
-    gu_step(near)
+    gu_step(right_hops)
+
+    def dn_step(k):
+        for st in dn:
+            for direction in (0, 1):
+                arrive(st, direction, k)
+
+    dn_step(1)
 
     def gu_sib(i, _):
         sib_arrive(gu, i)
         return 0
 
-    lax.fori_loop(0, far + 2, gu_sib, 0)
+    lax.fori_loop(0, left_hops + 2, gu_sib, 0)
     for d in range(n_tp - 1):
         arrival(nbuf.at[sources[d]], x_recv.at[1, d]).wait()
 
@@ -419,16 +426,11 @@
 
         lax.fori_loop(0, tiles, one, 0)
 
-    def dn_step(k):
-        for st in dn:
-            for direction in (0, 1):
-                arrive(st, direction, k)
-
-    offsets = [0] + [o for j in range(1, far) for o in (-j, j)] + [far]
+    offsets = [0] + [-j for j in range(1, right_hops + 1)] + list(range(1, left_hops + 1))
     group = -(-len(offsets) // 4)
     for k in range(4):
         accumulate(offsets[k * group:(k + 1) * group], k == 0, k == 3)
-        dn_step(k + 1)
+        dn_step(k + 2)
 
     def column_copy(d, at):
         return pltpu.make_async_remote_copy(
@@ -437,12 +439,12 @@
         )
 
     def down_step(j, _):
-        @pl.when(jnp.logical_and(j + 2 > 4, j + 2 <= far))
+        @pl.when(jnp.logical_and(lax.rem(j, 2) == 0, 6 + j // 2 <= left_hops))
         def _():
-            dn_step(j + 2)
+            dn_step(6 + j // 2)
 
         sib_arrive(dn, j)
-        back, ahead = chip(j), chip(-j)
+        back, ahead = chip(j), chip(jnp.where(j <= right_hops, -j, j))
         weights = jnp.concatenate(
             [dbuf[pl.ds(at * 2, 2)].reshape(2 * drow, ff) for at in (back, ahead)], axis=0
         )
@@ -452,7 +454,7 @@
         for d in range(n_tp - 1):
             column_copy(d, back).start()
 
-        @pl.when(jnp.logical_and(j >= 1, j <= near))
+        @pl.when(jnp.logical_and(j >= 1, j <= right_hops))
         def _():
             dsend[ahead] = y[:, :, 2 * drow:]
             for d in range(n_tp - 1):
@@ -460,7 +462,7 @@
 
         return 0
 
-    lax.fori_loop(0, far + 1, down_step, 0)
+    lax.fori_loop(0, left_hops + 1, down_step, 0)
 
     for d in range(n_tp - 1):
         arrival(drecv.at[sources[d]], x_recv.at[2, d]).wait()
@@ -553,8 +555,8 @@
             pltpu.VMEM((2 * heads, rows), F32),
             pltpu.VMEM((2 * heads, rows), F32),
             pltpu.SemaphoreType.DMA((6,)),
-            pltpu.SemaphoreType.DMA((6, 2, far + 1)),
-            pltpu.SemaphoreType.DMA((6, nz + far + 2)),
+            pltpu.SemaphoreType.DMA((6, 2, nz)),
+            pltpu.SemaphoreType.DMA((6, 2 * nz)),
             pltpu.SemaphoreType.DMA((7,)),
             pltpu.SemaphoreType.DMA((3,)),
             pltpu.SemaphoreType.DMA((3, n_tp - 1)),

time: 181 us -> 188 us (1.039)
  Pallas kernels: 177 us -> 185 us
    pallas_call x1, Pallas kernels: 177 us -> 185 us  [body(): pl.pallas_call(functools.partial(layer_kernel, n_sp, n_tp, heads), out_sh...]
where the time goes in v7:
time: 188 us
  Pallas kernels  185 us (98%)
  local copies, waits for them, and re-layouts  2.36 us (1%)
    pallas_call x1, Pallas kernels, body(): pl.pallas_call(functools.partial(layer_kernel, n_sp, n_tp, heads), out_sh...  185 us

profile of v7, /device:TPU:33, one launch (start us, length us, event | category | flops | bytes accessed | tf_op | source)
XLA Modules:
  0.0 188.2 jit_solution(17389255508446031054)
XLA Ops:
  0.0 0.0 copy-start
  0.0 0.1 pad.3.clone
  0.1 0.6 copy-done
  0.7 0.7 maximum_maximum_fusion.x_ref
  1.4 185.2 %shard_map.100 = bf16[64,2048]{1,0:T(8,128)(2,1)} custom-call(bf16[256,256]{1,0:T(8,128)(2,1)} %q_ref.1, bf16[256,256]{1,0:T(8,128)(2,1)} %k_ref.1, bf16[16,256]{1,0:T(8,128)(2,1)} %maximum_maximum_fusion.x_ref, bf16[256,256]{1,0:T(8,128)(2,1)} %v_ref.1, bf16[256,2048]{1,0:T(8,128)(2,1)} %res_ref.1, bf16[256,2048]{1,0:T(8,128)(2,1)} %wout_ref.1, ...), custom_call_target="tpu_custom_call" | custom-call | tf_op jit(solution)/shard_map/pallas_call | solution.py:526
  186.6 1.7 copy.12
  (2 shorter events, 0.0 us)
Async XLA Ops:
  0.0 0.7 copy-start

commit v8 on v3

--- a/solution.py
+++ b/solution.py
@@ -382,6 +382,13 @@
         send_own(st, 0)
     gu_step(near)
 
+    def dn_step(k):
+        for st in dn:
+            for direction in (0, 1):
+                arrive(st, direction, k)
+
+    dn_step(1)
+
     def gu_sib(i, _):
         sib_arrive(gu, i)
         return 0
@@ -419,16 +426,11 @@
 
         lax.fori_loop(0, tiles, one, 0)
 
-    def dn_step(k):
-        for st in dn:
-            for direction in (0, 1):
-                arrive(st, direction, k)
-
     offsets = [0] + [o for j in range(1, far) for o in (-j, j)] + [far]
     group = -(-len(offsets) // 4)
     for k in range(4):
         accumulate(offsets[k * group:(k + 1) * group], k == 0, k == 3)
-        dn_step(k + 1)
+        dn_step(k + 2)
 
     def column_copy(d, at):
         return pltpu.make_async_remote_copy(
@@ -437,9 +439,9 @@
         )
 
     def down_step(j, _):
-        @pl.when(jnp.logical_and(j + 2 > 4, j + 2 <= far))
+        @pl.when(jnp.logical_and(lax.rem(j, 3) == 0, 6 + j // 3 <= far))
         def _():
-            dn_step(j + 2)
+            dn_step(6 + j // 3)
 
         sib_arrive(dn, j)
         back, ahead = chip(j), chip(-j)

time: 181 us -> 179 us (0.989)
  no operation moved by 1% of the time
where the time goes in v8:
time: 179 us
  Pallas kernels  176 us (98%)
  local copies, waits for them, and re-layouts  2.36 us (1%)
    pallas_call x1, Pallas kernels, body(): pl.pallas_call(functools.partial(layer_kernel, n_sp, n_tp, heads), out_sh...  176 us

profile of v8, /device:TPU:33, one launch (start us, length us, event | category | flops | bytes accessed | tf_op | source)
XLA Modules:
  0.0 179.0 jit_solution(15678938768492954550)
XLA Ops:
  0.0 0.0 copy-start
  0.0 0.1 pad.3.clone
  0.1 0.6 copy-done
  0.7 0.7 maximum_maximum_fusion.x_ref
  1.4 176.0 %shard_map.100 = bf16[64,2048]{1,0:T(8,128)(2,1)} custom-call(bf16[256,256]{1,0:T(8,128)(2,1)} %q_ref.1, bf16[256,256]{1,0:T(8,128)(2,1)} %k_ref.1, bf16[16,256]{1,0:T(8,128)(2,1)} %maximum_maximum_fusion.x_ref, bf16[256,256]{1,0:T(8,128)(2,1)} %v_ref.1, bf16[256,2048]{1,0:T(8,128)(2,1)} %res_ref.1, bf16[256,2048]{1,0:T(8,128)(2,1)} %wout_ref.1, ...), custom_call_target="tpu_custom_call" | custom-call | tf_op jit(solution)/shard_map/pallas_call | solution.py:526
  177.4 1.7 copy.12
  (2 shorter events, 0.0 us)
Async XLA Ops:
  0.0 0.7 copy-start

commit v9 on v8

--- a/solution.py
+++ b/solution.py
@@ -358,12 +358,18 @@
     def arrival(buf, sem):
         return pltpu.make_async_copy(buf, buf, sem)
 
-    gu_step(3)
+    def gu_half(half, k):
+        arrive(gu[half], 0, k)
+        arrive(gu[half], 1, k + early)
+
+    gu_half(0, 3)
     for d in range(n_tp - 1):
         ready(4 + d)
         reduce_copy(d).start()
-    for k in range(4, near - 1):
+    gu_half(1, 3)
+    for k in range(4, near - 2):
         gu_step(k)
+    gu_half(0, near - 2)
     for d in range(n_tp - 1):
         arrival(rsbuf.at[sources[d]], x_recv.at[0, d]).wait()
     summed = resv[...].astype(F32) + pbuf[t].astype(F32)
@@ -376,6 +382,7 @@
     for d in range(n_tp - 1):
         gather_copy(d).start()
 
+    gu_half(1, near - 2)
     gu_step(near - 1)
     for st in dn:
         send_own(st, 1)

time: 179 us -> 179 us (level)
  no operation moved by 1% of the time
where the time goes in v9:
time: 179 us
  Pallas kernels  176 us (98%)
  local copies, waits for them, and re-layouts  2.36 us (1%)
    pallas_call x1, Pallas kernels, body(): pl.pallas_call(functools.partial(layer_kernel, n_sp, n_tp, heads), out_sh...  176 us

profile of v9, /device:TPU:33, one launch (start us, length us, event | category | flops | bytes accessed | tf_op | source)
XLA Modules:
  0.0 179.0 jit_solution(9973127654046234019)
XLA Ops:
  0.0 0.0 copy-start
  0.0 0.1 pad.3.clone
  0.1 0.6 copy-done
  0.7 0.7 maximum_maximum_fusion.x_ref
  1.4 176.0 %shard_map.100 = bf16[64,2048]{1,0:T(8,128)(2,1)} custom-call(bf16[256,256]{1,0:T(8,128)(2,1)} %q_ref.1, bf16[256,256]{1,0:T(8,128)(2,1)} %k_ref.1, bf16[16,256]{1,0:T(8,128)(2,1)} %maximum_maximum_fusion.x_ref, bf16[256,256]{1,0:T(8,128)(2,1)} %v_ref.1, bf16[256,2048]{1,0:T(8,128)(2,1)} %res_ref.1, bf16[256,2048]{1,0:T(8,128)(2,1)} %wout_ref.1, ...), custom_call_target="tpu_custom_call" | custom-call | tf_op jit(solution)/shard_map/pallas_call | solution.py:533
  177.4 1.7 copy.12
  (2 shorter events, 0.0 us)
Async XLA Ops:
  0.0 0.7 copy-start
